TPU v7x, 32 devices: a whole 2x2x4 slice. The times are simulated.
32 devices in a mesh: dp: 4 (over y, x), kv: 4 (over z), tp: 2 (over core).
Axes of the slice: x: 2, y: 2, z: 4, core: 2. Of those that a mesh axis runs over, the one named last changes fastest.
Arguments:
- piece_tokens: bfloat16 [2048, 2048], P(('dp', 'kv')), parts along dimension 0, may hold values from -6 to 6
- step_tokens: bfloat16 [16, 2048], P(('dp', 'kv')), parts along dimension 0, may hold values from -6 to 6
- norm_gain: float32 [2048], replicated, may hold values from 0.1 to 1.9
- query_weight: bfloat16 [2048, 1024], P(None, 'tp'), may hold values from -0.125 to 0.125
- key_weight: bfloat16 [2048, 1024], P(None, 'tp'), may hold values from -0.125 to 0.125
- value_weight: bfloat16 [2048, 1024], P(None, 'tp'), may hold values from -0.125 to 0.125
- gate_weight: bfloat16 [2048, 16], replicated, may hold values from -0.125 to 0.125
- gate_bias: float32 [16], replicated, may hold values from 3 to 10.5
- out_weight: bfloat16 [1024, 2048], P(None, 'tp'), may hold values from -0.1875 to 0.1875
- cache_keys: bfloat16 [8192, 1024], P(('dp', 'kv'), 'tp'), parts along dimension 0, may hold values from -320 to 320
- cache_values: bfloat16 [8192, 1024], P(('dp', 'kv'), 'tp'), parts along dimension 0, may hold values from -10 to 10
- cache_decay: float32 [16, 8192], P('tp', ('dp', 'kv')), parts along dimension 1, may hold values from -696.32 to 0, as said below
- decay_total: float32 [64], P('dp'), parts along dimension 0, may hold values from -696.32 to 0, as said below
- step_keys: bfloat16 [16, 1024, 1024], P(('dp', 'kv'), None, 'tp'), parts along dimension 0, may hold values from -6 to 6
- step_values: bfloat16 [16, 1024, 1024], P(('dp', 'kv'), None, 'tp'), parts along dimension 0, may hold values from -6 to 6
- step_gates: float32 [16, 16, 1024], P(('dp', 'kv'), 'tp'), parts along dimension 0, may hold values from -0.34 to 0
- step_lengths: int32 [16], P(('dp', 'kv')), parts along dimension 0, may hold values from 1 to 1024, 2048 in all
Outputs:
- piece_out: bfloat16 [2048, 2048], P(('dp', 'kv'), 'tp'), parts along dimension 0
- step_out: bfloat16 [16, 2048], P(('dp', 'kv'), 'tp'), parts along dimension 0
There are 4 independent parts, one for each index of `dp`. A program takes and returns all parts, laid end to end along the dimension named above; an argument that names none is the same for every part. Nothing has to cross between parts.
Inputs may be any that keep to these rules, and one draw needn't show every extreme that they name: `cache_decay`: cumulative values never rise along the positions and start at one gate below zero. `decay_total`: equal to the cumulative value of the last cached position. `step_lengths`: each length is 1 to 1024; the largest is exactly 1024; positions at or past a length are unused.
All inputs are finite; a program needn't handle non-finite values.
Results may differ from a plain program's by a relative error of at most 0.0095.
The roundings to bfloat16 on the way count: a program that leaves them out, or rounds other values in their place, can miss the bound.
Values may be sent and summed in bfloat16 or wider, within the bound.
A program may use at most 128 MiB of HBM per device.

v0:
```python
import functools
import math

import jax
import jax.numpy as jnp
from jax import lax
from jax.experimental import pallas as pl
from jax.experimental.pallas import tpu as pltpu
from jax.sharding import PartitionSpec as P

norm_eps = 1e-06
negative = -1e30
log2e = math.log2(math.e)
MESH = pl.DeviceIdType.MESH
F32 = jnp.float32
BF16 = jnp.bfloat16
NT = (((1,), (1,)), ((), ()))
TN = (((0,), (0,)), ((), ()))


chunk_count = 2


def iota(shape, dim):
    return lax.broadcasted_iota(jnp.int32, shape, dim)


def normalize(rows, gain):
    wide = rows.astype(F32)
    factor = lax.rsqrt(jnp.mean(wide * wide, axis=-1, keepdims=True) + norm_eps)
    return (wide * factor * gain).astype(BF16)


def to_column(row, count):
    eye = iota((count, count), 0) == iota((count, count), 1)
    return jnp.sum(jnp.where(eye, row, 0.0), axis=1, keepdims=True)


def kernel(
    n, heads, width,
    tok, stok, gain, gate_w, gate_b, total_decay, cache_decay, step_gates, step_len,
    wq, wk, wv, cache_k, cache_v, step_k, step_v,
    out_att,
    nrm, wq_v, wk_v, wv_v, k_all, k_turned, v_all, sk_v, sv_v,
    q_all, lg, gate_buf, key_bias, mean_buf, stat_buf, att, att_other,
    local_sem, q_right, q_left, q_recv, g_send, g_recv, m_send, m_recv, s_send, s_recv, x_send, x_recv,
):
    me = lax.axis_index("kv")
    tp = lax.axis_index("tp")
    rows = tok.shape[0]
    steps = stok.shape[0]
    cache_len = cache_k.shape[0]
    span = step_k.shape[0] // steps
    local = heads * width
    scale = width ** (-0.5) * log2e

    def fetch(index, src, dst):
        copy = pltpu.make_async_copy(src, dst, local_sem.at[index])
        copy.start()
        return copy

    c_wq = fetch(0, wq, wq_v)
    c_wk = fetch(1, wk, wk_v)
    c_wv = fetch(2, wv, wv_v)
    c_ck = fetch(3, cache_k, k_all)
    c_cv = fetch(4, cache_v, v_all.at[pl.ds(0, cache_len)])
    c_sk = fetch(5, step_k, sk_v)
    c_sv = fetch(6, step_v, sv_v)

    barrier = pltpu.get_barrier_semaphore()

    def greet(d, carry):
        pl.semaphore_signal(
            barrier, inc=1, device_id={"kv": lax.rem(me + d, n)}, device_id_type=MESH
        )
        return carry

    lax.fori_loop(1, n, greet, 0)
    pl.semaphore_signal(barrier, inc=1, device_id={"tp": 1 - tp}, device_id_type=MESH)

    nrm[pl.ds(0, rows)] = normalize(tok[...], gain[...])
    pad = nrm.shape[0] - rows
    step_norm = normalize(stok[...], gain[...]).astype(F32)
    step_rows = jnp.zeros((pad, nrm.shape[1]), F32)
    for b in range(steps):
        step_rows = jnp.where(iota((pad, nrm.shape[1]), 0) == b, step_norm[b : b + 1], step_rows)
    nrm[pl.ds(rows, pad)] = step_rows.astype(BF16)

    c_wq.wait()
    q_new = jnp.dot(nrm[...], wq_v[...], preferred_element_type=F32).astype(BF16)
    part = local // chunk_count
    for c in range(chunk_count):
        q_all[me, c] = q_new[:rows, c * part : (c + 1) * part]
    step_q = q_new[rows:].astype(F32)

    pl.semaphore_wait(barrier, n)

    def q_copy(source, c, step, sems):
        return pltpu.make_async_remote_copy(
            src_ref=q_all.at[source, c], dst_ref=q_all.at[source, c],
            send_sem=sems.at[source, c], recv_sem=q_recv.at[source, c],
            device_id={"kv": lax.rem(me + step + n, n)}, device_id_type=MESH,
        )

    def to_right(source, c):
        return q_copy(source, c, 1, q_right)

    def to_left(source, c):
        return q_copy(source, c, -1, q_left)

    has_right = me < n - 1
    has_left = me > 0

    def g_copy(d):
        return pltpu.make_async_remote_copy(
            src_ref=gate_buf.at[0], dst_ref=gate_buf.at[d],
            send_sem=g_send.at[d], recv_sem=g_recv.at[d],
            device_id={"kv": lax.rem(me + d, n)}, device_id_type=MESH,
        )

    def m_copy(d):
        return pltpu.make_async_remote_copy(
            src_ref=mean_buf.at[n + d], dst_ref=mean_buf.at[d],
            send_sem=m_send.at[d], recv_sem=m_recv.at[d],
            device_id={"kv": lax.rem(me + n - d, n)}, device_id_type=MESH,
        )

    def s_copy(d):
        return pltpu.make_async_remote_copy(
            src_ref=stat_buf.at[n + d], dst_ref=stat_buf.at[d],
            send_sem=s_send.at[d], recv_sem=s_recv.at[d],
            device_id={"kv": lax.rem(me + n - d, n)}, device_id_type=MESH,
        )

    def each(make):
        def body(d, carry):
            make(d)
            return carry

        lax.fori_loop(1, n, body, 0)

    for c in range(chunk_count):
        @pl.when(has_right)
        def _():
            to_right(me, c).start()

        @pl.when(has_left)
        def _():
            to_left(me, c).start()

    logits = lax.dot_general(gate_w[...], nrm[...], NT, preferred_element_type=F32)
    logits = logits + to_column(gate_b[...], gate_w.shape[0])
    lg[...] = jnp.minimum(logits, 0.0) - jnp.log1p(jnp.exp(-jnp.abs(logits)))
    own_lg = lg[pl.ds(pl.multiple_of(tp * heads, heads), heads), :]
    piece_lg = own_lg[:, :rows]
    gate_buf[0] = jnp.broadcast_to(jnp.sum(piece_lg, axis=1, keepdims=True), gate_buf.shape[1:])
    each(lambda d: g_copy(d).start())

    c_ck.wait()
    k_turned[:, pl.ds(0, cache_len)] = k_all[...].T
    c_wk.wait()
    k_new = jnp.dot(nrm[...], wk_v[...], preferred_element_type=F32).astype(BF16)
    k_turned[:, pl.ds(cache_len, rows)] = k_new[:rows].T
    step_nk = k_new[rows:].astype(F32)
    c_wv.wait()
    v_new = jnp.dot(nrm[...], wv_v[...], preferred_element_type=F32).astype(BF16)
    v_all[pl.ds(cache_len, rows)] = v_new[:rows]
    step_nv = v_new[rows:].astype(F32)

    upto = (iota((rows, rows), 0) <= iota((rows, rows), 1)).astype(F32)
    running = jnp.dot(
        piece_lg, upto, preferred_element_type=F32, precision=lax.Precision.HIGHEST
    )
    lg_start = to_column(total_decay[...], gate_w.shape[0])
    start_rows = jnp.where(tp == 0, lg_start[:heads], lg_start[heads : 2 * heads])
    key_bias[:, pl.ds(0, cache_len)] = (start_rows - cache_decay[...]) * log2e

    def add_before(d, total):
        g_copy(d).wait()
        return total + jnp.where(d <= me, gate_buf[d], 0.0)

    before = lax.fori_loop(1, n, add_before, jnp.zeros(gate_buf.shape[1:], F32))
    key_bias[:, pl.ds(cache_len, rows)] = -(before[:, :1] + running) * log2e

    pair_lanes = 2 * width
    low_lane = iota((rows, pair_lanes), 1) < width
    stat_lane = iota((rows, 128), 1)
    row_minus_col = iota((rows, rows), 0) - iota((rows, rows), 1)

    c_cv.wait()

    def attend(d, source, remote):
        slot = d + n if remote else d
        visible = row_minus_col >= (me - source) * rows
        stats = jnp.zeros((rows, 128), F32)
        pairs_in_part = heads // 2 // chunk_count
        for pair in range(heads // 2):
            lanes = pl.ds(pair * pair_lanes, pair_lanes)
            inner = pl.ds(pair % pairs_in_part * pair_lanes, pair_lanes)
            q_pair = q_all[source, pair // pairs_in_part, :, inner]
            keys = k_turned[lanes, :]
            values = v_all[:, lanes]
            outs = []
            for side in range(2):
                head = 2 * pair + side
                keep = low_lane if side == 0 else jnp.logical_not(low_lane)
                q_one = jnp.where(keep, q_pair, jnp.zeros_like(q_pair))
                scores = jnp.dot(q_one, keys, preferred_element_type=F32)
                scores = scores * scale + key_bias[head : head + 1, :]
                fresh = jnp.where(visible, scores[:, cache_len:], negative)
                scores = jnp.concatenate([scores[:, :cache_len], fresh], axis=1)
                high = jnp.max(scores, axis=1, keepdims=True)
                weight = jnp.exp2(scores - high)
                mass = jnp.sum(weight, axis=1, keepdims=True)
                mix = jnp.dot(weight.astype(BF16), values, preferred_element_type=F32)
                outs.append(mix / mass)
                stats = jnp.where(stat_lane == head, high, stats)
                stats = jnp.where(stat_lane == heads + head, mass, stats)
            mean_buf[slot, :, lanes] = jnp.where(low_lane, outs[0], outs[1]).astype(BF16)
        stat_buf[slot] = stats.T[: 2 * heads]
        if remote:
            m_copy(d).start()
            s_copy(d).start()

    def step(k, carry):
        for c in range(chunk_count):
            @pl.when(me >= k)
            def _():
                to_right(me - k, c).wait_recv()

                @pl.when(has_right)
                def _():
                    to_right(me - k, c).start()

            @pl.when(me + k < n)
            def _():
                to_left(me + k, c).wait_recv()

                @pl.when(has_left)
                def _():
                    to_left(me + k, c).start()

        @pl.when(me >= k)
        def _():
            attend(k, me - k, True)

        @pl.when(me + k < n)
        def _():
            attend(n - k, me + k, True)

        @pl.when(k == 1)
        def _():
            attend(0, me, False)

        return carry

    lax.fori_loop(1, n, step, 0)

    head_mask = lax.div(iota((heads, local), 1), width) == iota((heads, local), 0)
    chunk = 128
    chunks = span // chunk
    later = (iota((chunk, chunk), 0) > iota((chunk, chunk), 1)).astype(F32)
    c_sk.wait()
    c_sv.wait()
    step_att = jnp.zeros((pad, local), F32)
    for b in range(steps):
        length = step_len[b]
        in_cache = iota((heads, span), 1) < length
        kept = jnp.where(in_cache, step_gates[b], 0.0)
        tail = jnp.zeros((heads, 1), F32)
        parts = [None] * chunks
        for c in reversed(range(chunks)):
            piece = kept[:, c * chunk : (c + 1) * chunk]
            inner = jnp.dot(
                piece, later, preferred_element_type=F32, precision=lax.Precision.HIGHEST
            )
            parts[c] = inner + tail
            tail = tail + jnp.sum(piece, axis=1, keepdims=True)
        after = jnp.concatenate(parts, axis=1)
        q_row = jnp.where(head_mask, step_q[b : b + 1], 0.0)
        scores = lax.dot_general(
            q_row.astype(BF16), sk_v[pl.ds(b * span, span)], NT, preferred_element_type=F32
        )
        new_lg = own_lg[:, rows + b : rows + b + 1]
        scores = scores * scale + (new_lg + after) * log2e
        scores = jnp.where(in_cache, scores, negative)
        self_score = jnp.sum(q_row * step_nk[b : b + 1], axis=1, keepdims=True) * scale
        high = jnp.maximum(jnp.max(scores, axis=1, keepdims=True), self_score)
        weight = jnp.exp2(scores - high)
        self_weight = jnp.exp2(self_score - high)
        mass = jnp.sum(weight, axis=1, keepdims=True) + self_weight
        mix = jnp.dot(
            weight.astype(BF16), sv_v[pl.ds(b * span, span)], preferred_element_type=F32
        )
        mix = mix + self_weight.astype(BF16).astype(F32) * step_nv[b : b + 1]
        one = jnp.sum(jnp.where(head_mask, mix / mass, 0.0), axis=0, keepdims=True)
        step_att = jnp.where(iota((pad, local), 0) == b, one, step_att)
    att[pl.ds(rows, pad)] = step_att.astype(BF16)

    def top(d, best):
        s_copy(d).wait()
        return jnp.maximum(best, stat_buf[d, :heads])

    best = lax.fori_loop(1, n, top, stat_buf[0, :heads])

    def share_of(d):
        return stat_buf[d, pl.ds(heads, heads)] * jnp.exp2(stat_buf[d, :heads] - best)

    total = lax.fori_loop(1, n, lambda d, t: t + share_of(d), share_of(0))
    spread = head_mask.astype(F32)

    def weighted(d):
        wide = lax.dot_general(
            share_of(d) / total, spread, TN,
            preferred_element_type=F32, precision=lax.Precision.HIGHEST,
        )
        return wide * mean_buf[d].astype(F32)

    def add_block(d, acc):
        m_copy(d).wait()
        return acc + weighted(d)

    att[pl.ds(0, rows)] = lax.fori_loop(1, n, add_block, weighted(0)).astype(BF16)

    swap = pltpu.make_async_remote_copy(
        src_ref=att, dst_ref=att_other, send_sem=x_send, recv_sem=x_recv,
        device_id={"tp": 1 - tp}, device_id_type=MESH,
    )
    swap.start()
    mine = pl.ds(pl.multiple_of(tp * local, local), local)
    other = pl.ds(pl.multiple_of((1 - tp) * local, local), local)
    out_att[:, mine] = att[...]
    swap.wait()
    out_att[:, other] = att_other[...]

    def sent(source, carry):
        for c in range(chunk_count):
            @pl.when(jnp.logical_and(has_right, source <= me))
            def _():
                to_right(source, c).wait_send()

            @pl.when(jnp.logical_and(has_left, source >= me))
            def _():
                to_left(source, c).wait_send()

        return carry

    lax.fori_loop(0, n, sent, 0)


def project(rows, att, weight, out_piece, out_step):
    projected = jnp.dot(att[...], weight[...], preferred_element_type=F32)
    out_piece[...] = projected[:rows].astype(BF16)
    out_step[...] = projected[rows : rows + out_step.shape[0]].astype(BF16)


def per_device(
    piece_tokens, step_tokens, norm_gain, query_weight, key_weight, value_weight,
    gate_weight, gate_bias, out_weight, cache_keys, cache_values, cache_decay,
    decay_total, step_keys, step_values, step_gates, step_lengths,
):
    n = lax.axis_size("kv")
    rows, model = piece_tokens.shape
    steps = step_tokens.shape[0]
    heads = cache_decay.shape[0]
    local = query_weight.shape[1]
    width = local // heads
    cache_len = cache_keys.shape[0]
    span = step_keys.shape[1]
    columns = out_weight.shape[1]
    padded = rows + 16 * (-(-steps // 16))
    vmem = pl.BlockSpec(memory_space=pltpu.VMEM)
    smem = pl.BlockSpec(memory_space=pltpu.SMEM)
    hbm = pl.BlockSpec(memory_space=pltpu.HBM)
    dma = pltpu.SemaphoreType.DMA
    att = pl.pallas_call(
        functools.partial(kernel, n, heads, width),
        out_shape=jax.ShapeDtypeStruct((padded, out_weight.shape[0]), BF16),
        in_specs=[vmem] * 8 + [smem] + [hbm] * 7,
        out_specs=vmem,
        scratch_shapes=[
            pltpu.VMEM((padded, model), BF16),
            pltpu.VMEM(query_weight.shape, BF16),
            pltpu.VMEM(key_weight.shape, BF16),
            pltpu.VMEM(value_weight.shape, BF16),
            pltpu.VMEM((cache_len, local), BF16),
            pltpu.VMEM((local, cache_len + rows), BF16),
            pltpu.VMEM((cache_len + rows, local), BF16),
            pltpu.VMEM((steps * span, local), BF16),
            pltpu.VMEM((steps * span, local), BF16),
            pltpu.VMEM((n, chunk_count, rows, local // chunk_count), BF16),
            pltpu.VMEM((gate_weight.shape[1], padded), F32),
            pltpu.VMEM((n, heads, 128), F32),
            pltpu.VMEM((heads, cache_len + rows), F32),
            pltpu.VMEM((2 * n, rows, local), BF16),
            pltpu.VMEM((2 * n, 2 * heads, rows), F32),
            pltpu.VMEM((padded, local), BF16),
            pltpu.VMEM((padded, local), BF16),
            dma((7,)),
            dma((n, chunk_count)), dma((n, chunk_count)), dma((n, chunk_count)),
            dma((n,)), dma((n,)),
            dma((n,)), dma((n,)), dma((n,)), dma((n,)),
            dma(()), dma(()),
        ],
        compiler_params=pltpu.CompilerParams(
            collective_id=0, has_side_effects=True, vmem_limit_bytes=60 * 1024 * 1024
        ),
    )(
        piece_tokens, step_tokens, norm_gain.reshape(1, -1), gate_weight.T,
        gate_bias.reshape(1, -1), decay_total.reshape(1, -1), cache_decay, step_gates,
        step_lengths, query_weight, key_weight, value_weight,
        cache_keys, cache_values,
        step_keys.reshape(steps * span, local), step_values.reshape(steps * span, local),
    )
    return pl.pallas_call(
        functools.partial(project, rows),
        out_shape=(
            jax.ShapeDtypeStruct((rows, columns), BF16),
            jax.ShapeDtypeStruct((steps, columns), BF16),
        ),
        in_specs=[vmem, vmem],
        out_specs=(vmem, vmem),
        compiler_params=pltpu.CompilerParams(vmem_limit_bytes=16 * 1024 * 1024),
    )(att, out_weight)


def solution(mesh):
    rows = P(("dp", "kv"), None)
    both = P(("dp", "kv"), "tp")
    cols = P(None, "tp")
    in_specs = (
        rows, rows, P(), cols, cols, cols, P(), P(), cols, both, both,
        P("tp", ("dp", "kv")), P("dp"),
        P(("dp", "kv"), None, "tp"), P(("dp", "kv"), None, "tp"),
        P(("dp", "kv"), "tp", None), P(("dp", "kv")),
    )
    return jax.shard_map(
        per_device, mesh=mesh, in_specs=in_specs, out_specs=(both, both), check_vma=False
    )
```

profile of v0, /device:TPU:0, one launch (start us, length us, event | category | flops | bytes accessed | tf_op | source)
XLA Modules:
  0.0 38.9 jit_solution(4513510373686740028)
XLA Ops:
  1.3 0.0 copy-start
  1.3 35.4 %shard_map.176.att = bf16[144,1024]{1,0:T(8,128)(2,1)} custom-call(bf16[128,2048]{1,0:T(8,128)(2,1)} %tok.1, bf16[1,2048]{1,0:T(2,128)(2,1)} %stok.1, f32[1,2048]{1,0:T(1,128)} %bitcast.9, bf16[16,2048]{1,0:T(8,128)(2,1)} %bitcast.8, f32[1,16]{1,0:T(1,128)} %bitcast.10, f32[1,16]{1,0:T(1,128)} %bitcast.11, f32[8,512]{1,0:T(8,128)} %cache_decay.1, ...), custom_call_target="tpu_custom_call" | custom-call | tf_op jit(solution)/shard_map/pallas_call | solution.py:376
  36.7 0.0 copy-done
  36.7 0.0 copy-start.1
  36.7 1.0 %copy-done.1 = bf16[144,1024]{1,0:T(8,128)(2,1)S(1)} copy-done((bf16[144,1024]{1,0:T(8,128)(2,1)S(1)}, bf16[144,1024]{1,0:T(8,128)(2,1)}, u32[]{:S(2)}) %copy-start.1) | copy-done | bytes 294936
  37.7 1.2 %shard_map.177 = (bf16[128,1024]{1,0:T(8,128)(2,1)}, bf16[1,1024]{1,0:T(2,128)(2,1)}) custom-call(bf16[144,1024]{1,0:T(8,128)(2,1)S(1)} %copy-done.1, bf16[1024,1024]{1,0:T(8,128)(2,1)S(1)} %copy-done), custom_call_target="tpu_custom_call" | custom-call | tf_op jit(solution)/shard_map/pallas_call | solution.py:415
Async XLA Ops:
  1.3 35.4 %copy-start = (bf16[1024,1024]{1,0:T(8,128)(2,1)S(1)}, bf16[1024,1024]{1,0:T(8,128)(2,1)}, u32[]{:S(2)}) copy-start(bf16[1024,1024]{1,0:T(8,128)(2,1)} %weight.1) | copy-start | bytes 6291460
  36.7 1.0 %copy-start.1 = (bf16[144,1024]{1,0:T(8,128)(2,1)S(1)}, bf16[144,1024]{1,0:T(8,128)(2,1)}, u32[]{:S(2)}) copy-start(bf16[144,1024]{1,0:T(8,128)(2,1)} %shard_map.176.att) | copy-start | bytes 884740
where the time goes:
time: 39.1 us; the launch traced here: 38.9 us
  Pallas kernels  36.6 us (94%)
  between operations  1.32 us (3%)
  local copies, waits for them, and re-layouts  0.96 us (2%)
    pallas_call x1, Pallas kernels, per_device(): pl.pallas_call(functools.partial(kernel, n, heads, width), out_shape=jax....  35.4 us
    pallas_call x1, Pallas kernels, per_device(): pl.pallas_call(functools.partial(project, rows), out_shape=(jax.ShapeDtyp...  1.19 us
    unnamed x4, local copies, waits for them, and re-layouts  0.96 us

commit v1 on v0

v1 whole, which is shorter than its diff:
```python
import functools
import math

import jax
import jax.numpy as jnp
from jax import lax
from jax.experimental import pallas as pl
from jax.experimental.pallas import tpu as pltpu
from jax.sharding import PartitionSpec as P

norm_eps = 1e-06
negative = -1e30
log2e = math.log2(math.e)
MESH = pl.DeviceIdType.MESH
F32 = jnp.float32
BF16 = jnp.bfloat16
NT = (((1,), (1,)), ((), ()))


def iota(shape, dim):
    return lax.broadcasted_iota(jnp.int32, shape, dim)


def normalize(rows, gain):
    wide = rows.astype(F32)
    factor = lax.rsqrt(jnp.mean(wide * wide, axis=-1, keepdims=True) + norm_eps)
    return (wide * factor * gain).astype(BF16)


def to_column(row, count):
    eye = iota((count, count), 0) == iota((count, count), 1)
    return jnp.sum(jnp.where(eye, row, 0.0), axis=1, keepdims=True)


def kernel(
    n, heads, width,
    tok_h, stok_h, gain_h, gate_w_h, gate_b_h, total_h, cache_decay_h, step_gates_h, step_len_h,
    wq, wk, wv, cache_k, cache_v, step_k, step_v, w_out,
    out_piece, out_step,
    tok, stok, gain, gate_w, gate_b, total_decay, cache_decay, step_gates, step_len,
    nrm, wq_v, wk_v, wv_v, k_all, cv_v, v_turned, sk_v, sv_v, wo_v,
    q_all, lg, gate_in, gate_out, bias_rows, bias_lanes, picks,
    own_mean, own_stat, to_r, to_l, stat_r, stat_l, own_final, own_final_stat, att,
    local_sem, q_right, q_left, q_recv, g_send, g_recv,
    m_send, m_recv, s_send, s_recv, x_send, x_recv,
):
    me = lax.axis_index("kv")
    tp = lax.axis_index("tp")
    rows = tok.shape[0]
    steps = stok.shape[0]
    cache_len = cache_k.shape[0]
    span = step_k.shape[0] // steps
    local = heads * width
    pair_lanes = 2 * width
    pairs = heads // 2
    keys = cache_len + rows
    root = math.sqrt(width)
    scale = log2e / root

    count = [0]

    def fetch(src, dst):
        copy = pltpu.make_async_copy(src, dst, local_sem.at[count[0]])
        count[0] += 1
        copy.start()
        return copy

    halves = 2 if local % 256 == 0 else 1
    part = local // halves
    c_tok = fetch(tok_h, tok)
    c_gain = fetch(gain_h, gain)
    c_stok = fetch(stok_h, stok)
    c_wq = [
        fetch(wq.at[:, pl.ds(c * part, part)], wq_v.at[:, pl.ds(c * part, part)])
        for c in range(halves)
    ]
    c_gw = fetch(gate_w_h, gate_w)
    c_gb = fetch(gate_b_h, gate_b)
    c_wk = fetch(wk, wk_v)
    c_wv = fetch(wv, wv_v)
    c_ck = fetch(cache_k, k_all.at[pl.ds(0, cache_len)])
    c_cv = fetch(cache_v, cv_v)
    c_td = fetch(total_h, total_decay)
    c_cd = fetch(cache_decay_h, cache_decay)
    c_sk = fetch(step_k, sk_v)
    c_sv = fetch(step_v, sv_v)
    c_sg = fetch(step_gates_h, step_gates)
    c_sl = fetch(step_len_h, step_len)
    c_wo = fetch(w_out, wo_v)

    has_right = me < n - 1
    has_left = me > 0
    right = lax.rem(me + 1, n)
    left = lax.rem(me + n - 1, n)

    barrier = pltpu.get_barrier_semaphore()

    @pl.when(has_right)
    def _():
        pl.semaphore_signal(barrier, inc=1, device_id={"kv": right}, device_id_type=MESH)

    @pl.when(has_left)
    def _():
        pl.semaphore_signal(barrier, inc=1, device_id={"kv": left}, device_id_type=MESH)

    pl.semaphore_signal(barrier, inc=1, device_id={"tp": 1 - tp}, device_id_type=MESH)

    def q_copy(source, p, sems, target):
        return pltpu.make_async_remote_copy(
            src_ref=q_all.at[source, p], dst_ref=q_all.at[source, p],
            send_sem=sems.at[source, p], recv_sem=q_recv.at[source, p],
            device_id={"kv": target}, device_id_type=MESH,
        )

    def q_to_right(source, p):
        return q_copy(source, p, q_right, right)

    def q_to_left(source, p):
        return q_copy(source, p, q_left, left)

    def part_copies(side, owner, p):
        means, stats, target = (to_r, stat_r, right) if side == 0 else (to_l, stat_l, left)
        return [
            pltpu.make_async_remote_copy(
                src_ref=ref.at[owner, p], dst_ref=ref.at[owner, p],
                send_sem=send.at[side, owner, p], recv_sem=recv.at[side, owner, p],
                device_id={"kv": target}, device_id_type=MESH,
            )
            for ref, send, recv in ((means, m_send, m_recv), (stats, s_send, s_recv))
        ]

    def send_part(side, owner, p):
        for copy in part_copies(side, owner, p):
            copy.start()

    def wait_part(side, owner, p):
        for copy in part_copies(side, owner, p):
            copy.wait_recv()

    c_tok.wait()
    c_gain.wait()
    c_stok.wait()
    nrm[pl.ds(0, rows)] = normalize(tok[...], gain[...])
    pad = nrm.shape[0] - rows
    step_norm = normalize(stok[...], gain[...]).astype(F32)
    step_rows = jnp.zeros((pad, nrm.shape[1]), F32)
    for b in range(steps):
        step_rows = jnp.where(iota((pad, nrm.shape[1]), 0) == b, step_norm[b : b + 1], step_rows)
    nrm[pl.ds(rows, pad)] = step_rows.astype(BF16)

    pairs_in_part = part // pair_lanes
    step_q_parts = []
    for c in range(halves):
        c_wq[c].wait()
        q_new = jnp.dot(
            nrm[...], wq_v[:, c * part : (c + 1) * part], preferred_element_type=F32
        ).astype(BF16)
        turned = q_new[:rows].T
        for i in range(pairs_in_part):
            q_all[me, c * pairs_in_part + i] = turned[i * pair_lanes : (i + 1) * pair_lanes]
        step_q_parts.append(q_new[rows:].astype(F32))
        if c == 0:
            pl.semaphore_wait(
                barrier, 1 + has_right.astype(jnp.int32) + has_left.astype(jnp.int32)
            )
        for i in range(pairs_in_part):
            p = c * pairs_in_part + i

            @pl.when(has_right)
            def _():
                q_to_right(me, p).start()

            @pl.when(has_left)
            def _():
                q_to_left(me, p).start()

    step_q = jnp.concatenate(step_q_parts, axis=1)

    c_gw.wait()
    c_gb.wait()
    logits = lax.dot_general(gate_w[...], nrm[...], NT, preferred_element_type=F32)
    logits = logits + to_column(gate_b[...], gate_w.shape[0])
    lg[...] = jnp.minimum(logits, 0.0) - jnp.log1p(jnp.exp(-jnp.abs(logits)))
    own_lg = lg[pl.ds(pl.multiple_of(tp * heads, heads), heads), :]
    piece_lg = own_lg[:, :rows]
    own_sum = jnp.broadcast_to(jnp.sum(piece_lg, axis=1, keepdims=True), gate_out.shape)

    g_copy = pltpu.make_async_remote_copy(
        src_ref=gate_out, dst_ref=gate_in, send_sem=g_send, recv_sem=g_recv,
        device_id={"kv": right}, device_id_type=MESH,
    )

    @pl.when(jnp.logical_not(has_left))
    def _():
        gate_in[...] = jnp.zeros(gate_in.shape, F32)
        gate_out[...] = own_sum

        @pl.when(has_right)
        def _():
            g_copy.start()

    c_wk.wait()
    k_new = jnp.dot(nrm[...], wk_v[...], preferred_element_type=F32).astype(BF16)
    k_all[pl.ds(cache_len, rows)] = k_new[:rows]
    step_nk = k_new[rows:].astype(F32)
    c_wv.wait()
    v_new = jnp.dot(nrm[...], wv_v[...], preferred_element_type=F32).astype(BF16)
    v_turned[:, pl.ds(cache_len, rows)] = v_new[:rows].T
    step_nv = v_new[rows:].astype(F32)
    c_cv.wait()
    v_turned[:, pl.ds(0, cache_len)] = cv_v[...].T

    upto = (iota((rows, rows), 0) <= iota((rows, rows), 1)).astype(F32)
    running = jnp.dot(
        piece_lg, upto, preferred_element_type=F32, precision=lax.Precision.HIGHEST
    )

    def bias_terms(bias):
        high = bias.astype(BF16).astype(F32)
        rest = bias - high
        middle = rest.astype(BF16).astype(F32)
        low = rest - middle
        blank = jnp.zeros((128 - 3 * heads, bias.shape[1]), F32)
        return jnp.concatenate([high, middle, low, blank], axis=0).T.astype(BF16)

    c_td.wait()
    c_cd.wait()
    lg_start = to_column(total_decay[...], gate_w.shape[0])
    start_rows = jnp.where(tp == 0, lg_start[:heads], lg_start[heads : 2 * heads])
    bias_lanes[pl.ds(0, cache_len)] = bias_terms((start_rows - cache_decay[...]) * root)
    bias_rows[...] = running

    head_of_column = lax.div(iota((128, 2 * rows), 1), rows)
    lane_of_term = iota((128, 2 * rows), 0)
    for p in range(pairs):
        hit = jnp.logical_and(
            lax.rem(lane_of_term, heads) == 2 * p + head_of_column, lane_of_term < 3 * heads
        )
        picks[p] = hit.astype(F32).astype(BF16)

    def finish_bias():
        @pl.when(has_left)
        def _():
            g_copy.wait_recv()

            @pl.when(has_right)
            def _():
                gate_out[...] = gate_in[...] + own_sum
                g_copy.start()

        fresh = -(gate_in[:, :1] + bias_rows[...]) * root
        bias_lanes[pl.ds(cache_len, rows)] = bias_terms(fresh)

    @pl.when(has_right)
    def _():
        finish_bias()

    c_ck.wait()

    first_rows = iota((pair_lanes, rows), 0) < width
    causal = lax.rem(iota((rows, 2 * rows), 1), rows) >= iota((rows, 2 * rows), 0)

    def spread(two):
        return jnp.concatenate(
            [
                jnp.broadcast_to(two[0:1], (width, rows)),
                jnp.broadcast_to(two[1:2], (width, rows)),
            ],
            axis=0,
        )

    def attend(source, p, used, masked):
        q_pair = q_all[source, p]
        zero = jnp.zeros_like(q_pair)
        rhs = jnp.concatenate(
            [
                jnp.concatenate(
                    [jnp.where(first_rows, q_pair, zero), jnp.where(first_rows, zero, q_pair)],
                    axis=1,
                ),
                picks[p],
            ],
            axis=0,
        )
        lanes = pl.ds(p * pair_lanes, pair_lanes)
        lhs = jnp.concatenate([k_all[pl.ds(0, used), lanes], bias_lanes[pl.ds(0, used)]], axis=1)
        raw = jnp.dot(lhs, rhs, preferred_element_type=F32)
        if masked:
            fresh = jnp.where(causal, raw[cache_len:], negative)
            raw = jnp.concatenate([raw[:cache_len], fresh], axis=0)
        high = jnp.max(raw, axis=0, keepdims=True)
        weight = jnp.exp2((raw - high) * scale)
        mass = jnp.sum(weight, axis=0, keepdims=True)
        mix = jnp.dot(
            v_turned[lanes, pl.ds(0, used)], weight.astype(BF16), preferred_element_type=F32
        )
        mix = mix * (1.0 / mass)
        mean = jnp.concatenate([mix[:width, :rows], mix[width:, rows:]], axis=0)
        level = high * scale + jnp.log2(mass)
        return mean, jnp.concatenate([level[:, :rows], level[:, rows:]], axis=0)

    def merge(pieces):
        best = functools.reduce(jnp.maximum, [level for _, level in pieces])
        shares = [jnp.exp2(level - best) for _, level in pieces]
        total = functools.reduce(jnp.add, shares)
        inverse = 1.0 / total
        mean = functools.reduce(
            jnp.add,
            [spread(share * inverse) * mean for share, (mean, _) in zip(shares, pieces)],
        )
        return mean, best + jnp.log2(total)

    def attend_left(k, p):
        source = me - k
        q_to_right(source, p).wait_recv()

        @pl.when(has_right)
        def _():
            q_to_right(source, p).start()

        mean, level = attend(source, p, cache_len, False)

        @pl.when(has_right)
        def _():
            own_mean[source, p] = mean
            own_stat[source, p] = level

        @pl.when(jnp.logical_not(has_right))
        def _():
            to_l[source, p] = mean.astype(BF16)
            stat_l[source, p] = level
            send_part(1, source, p)

    def attend_right(k, p):
        source = me + k
        q_to_left(source, p).wait_recv()

        @pl.when(has_left)
        def _():
            q_to_left(source, p).start()

        mean, level = attend(source, p, keys, False)

        @pl.when(has_left)
        def _():
            own_mean[source, p] = mean
            own_stat[source, p] = level

        @pl.when(jnp.logical_not(has_left))
        def _():
            to_r[source, p] = mean.astype(BF16)
            stat_r[source, p] = level
            send_part(0, source, p)

    def attend_own():
        @pl.when(jnp.logical_not(has_right))
        def _():
            finish_bias()

        for p in range(pairs):
            mean, level = attend(me, p, keys, True)
            own_final[p] = mean
            own_final_stat[p] = level

    def decode():
        head_mask = lax.div(iota((heads, local), 1), width) == iota((heads, local), 0)
        chunk = 128
        chunks = span // chunk
        later = (iota((chunk, chunk), 0) > iota((chunk, chunk), 1)).astype(F32)
        c_sk.wait()
        c_sv.wait()
        c_sg.wait()
        c_sl.wait()
        step_att = jnp.zeros((pad, local), F32)
        for b in range(steps):
            length = step_len[b]
            in_cache = iota((heads, span), 1) < length
            kept = jnp.where(in_cache, step_gates[b], 0.0)
            tail = jnp.zeros((heads, 1), F32)
            parts = [None] * chunks
            for c in reversed(range(chunks)):
                piece = kept[:, c * chunk : (c + 1) * chunk]
                inner = jnp.dot(
                    piece, later, preferred_element_type=F32, precision=lax.Precision.HIGHEST
                )
                parts[c] = inner + tail
                tail = tail + jnp.sum(piece, axis=1, keepdims=True)
            after = jnp.concatenate(parts, axis=1)
            q_row = jnp.where(head_mask, step_q[b : b + 1], 0.0)
            scores = lax.dot_general(
                q_row.astype(BF16), sk_v[pl.ds(b * span, span)], NT, preferred_element_type=F32
            )
            new_lg = own_lg[:, rows + b : rows + b + 1]
            scores = scores * scale + (new_lg + after) * log2e
            scores = jnp.where(in_cache, scores, negative)
            self_score = jnp.sum(q_row * step_nk[b : b + 1], axis=1, keepdims=True) * scale
            high = jnp.maximum(jnp.max(scores, axis=1, keepdims=True), self_score)
            weight = jnp.exp2(scores - high)
            self_weight = jnp.exp2(self_score - high)
            mass = jnp.sum(weight, axis=1, keepdims=True) + self_weight
            mix = jnp.dot(
                weight.astype(BF16), sv_v[pl.ds(b * span, span)], preferred_element_type=F32
            )
            mix = mix + self_weight.astype(BF16).astype(F32) * step_nv[b : b + 1]
            one = jnp.sum(jnp.where(head_mask, mix / mass, 0.0), axis=0, keepdims=True)
            step_att = jnp.where(iota((pad, local), 0) == b, one, step_att)
        done = step_att.astype(BF16)
        for p in range(pairs):
            att[tp * pairs + p, pl.ds(rows, pad)] = done[:, p * pair_lanes : (p + 1) * pair_lanes]

    def step(k, carry):
        for p in range(pairs):
            @pl.when(me >= k)
            def _():
                attend_left(k, p)

            @pl.when(me + k < n)
            def _():
                attend_right(k, p)

        @pl.when(k == 1)
        def _():
            decode()

        @pl.when(k == min(2, n - 1))
        def _():
            attend_own()

        return carry

    lax.fori_loop(1, n, step, 0)

    def forward(side, owner, p):
        wait_part(side, owner, p)
        means, stats = (to_r, stat_r) if side == 0 else (to_l, stat_l)
        mean, level = merge(
            [
                (means[owner, p].astype(F32), stats[owner, p]),
                (own_mean[owner, p], own_stat[owner, p]),
            ]
        )
        means[owner, p] = mean.astype(BF16)
        stats[owner, p] = level
        send_part(side, owner, p)

    def pass_right(r):
        @pl.when(jnp.logical_and(has_left, r > me))
        def _():
            for p in range(pairs):
                forward(0, r, p)

    def pass_left(r):
        owner = n - 1 - r

        @pl.when(jnp.logical_and(has_right, owner < me))
        def _():
            for p in range(pairs):
                forward(1, owner, p)

    def turn(r, carry):
        @pl.when(2 * me < n)
        def _():
            pass_right(r)
            pass_left(r)

        @pl.when(2 * me >= n)
        def _():
            pass_left(r)
            pass_right(r)

        return carry

    lax.fori_loop(1, n, turn, 0)

    def swap(p):
        slot = tp * pairs + p
        return pltpu.make_async_remote_copy(
            src_ref=att.at[slot], dst_ref=att.at[slot],
            send_sem=x_send.at[p], recv_sem=x_recv.at[p],
            device_id={"tp": 1 - tp}, device_id_type=MESH,
        )

    def swap_in(p):
        slot = (1 - tp) * pairs + p
        return pltpu.make_async_remote_copy(
            src_ref=att.at[slot], dst_ref=att.at[slot],
            send_sem=x_send.at[p], recv_sem=x_recv.at[p],
            device_id={"tp": 1 - tp}, device_id_type=MESH,
        )

    def finish(p, sides):
        pieces = [(own_final[p], own_final_stat[p])]
        for side in sides:
            wait_part(side, me, p)
            means, stats = (to_r, stat_r) if side == 0 else (to_l, stat_l)
            pieces.append((means[me, p].astype(F32), stats[me, p]))
        mean, _ = merge(pieces)
        att[tp * pairs + p, pl.ds(0, rows)] = mean.T.astype(BF16)
        swap(p).start()

    @pl.when(jnp.logical_and(has_left, has_right))
    def _():
        for p in range(pairs):
            finish(p, (0, 1))

    @pl.when(jnp.logical_and(has_left, jnp.logical_not(has_right)))
    def _():
        for p in range(pairs):
            finish(p, (0,))

    @pl.when(jnp.logical_and(has_right, jnp.logical_not(has_left)))
    def _():
        for p in range(pairs):
            finish(p, (1,))

    c_wo.wait()
    for p in range(pairs):
        swap_in(p).wait_recv()
    whole = jnp.concatenate([att[i] for i in range(2 * pairs)], axis=1)
    projected = jnp.dot(whole, wo_v[...], preferred_element_type=F32)
    out_piece[...] = projected[:rows].astype(BF16)
    out_step[...] = projected[rows : rows + steps].astype(BF16)

    for p in range(pairs):
        swap(p).wait_send()

    @pl.when(has_right)
    def _():
        g_copy.wait_send()

    def sent(owner, carry):
        for p in range(pairs):
            @pl.when(jnp.logical_and(has_right, owner <= me))
            def _():
                q_to_right(owner, p).wait_send()

            @pl.when(jnp.logical_and(has_left, owner >= me))
            def _():
                q_to_left(owner, p).wait_send()

            @pl.when(owner > me)
            def _():
                for copy in part_copies(0, owner, p):
                    copy.wait_send()

            @pl.when(owner < me)
            def _():
                for copy in part_copies(1, owner, p):
                    copy.wait_send()

        return carry

    lax.fori_loop(0, n, sent, 0)


def per_device(
    piece_tokens, step_tokens, norm_gain, query_weight, key_weight, value_weight,
    gate_weight, gate_bias, out_weight, cache_keys, cache_values, cache_decay,
    decay_total, step_keys, step_values, step_gates, step_lengths,
):
    n = lax.axis_size("kv")
    rows, model = piece_tokens.shape
    steps = step_tokens.shape[0]
    heads = cache_decay.shape[0]
    local = query_weight.shape[1]
    width = local // heads
    pairs = heads // 2
    cache_len = cache_keys.shape[0]
    keys = cache_len + rows
    span = step_keys.shape[1]
    columns = out_weight.shape[1]
    padded = rows + 16 * (-(-steps // 16))
    all_heads = gate_weight.shape[1]
    vmem = pl.BlockSpec(memory_space=pltpu.VMEM)
    hbm = pl.BlockSpec(memory_space=pltpu.HBM)
    dma = pltpu.SemaphoreType.DMA
    return pl.pallas_call(
        functools.partial(kernel, n, heads, width),
        out_shape=(
            jax.ShapeDtypeStruct((rows, columns), BF16),
            jax.ShapeDtypeStruct((steps, columns), BF16),
        ),
        in_specs=[hbm] * 17,
        out_specs=(vmem, vmem),
        scratch_shapes=[
            pltpu.VMEM((rows, model), BF16),
            pltpu.VMEM((steps, model), BF16),
            pltpu.VMEM((1, model), F32),
            pltpu.VMEM((all_heads, model), BF16),
            pltpu.VMEM((1, all_heads), F32),
            pltpu.VMEM((1, all_heads), F32),
            pltpu.VMEM(cache_decay.shape, F32),
            pltpu.VMEM(step_gates.shape, F32),
            pltpu.SMEM((steps,), jnp.int32),
            pltpu.VMEM((padded, model), BF16),
            pltpu.VMEM(query_weight.shape, BF16),
            pltpu.VMEM(key_weight.shape, BF16),
            pltpu.VMEM(value_weight.shape, BF16),
            pltpu.VMEM((keys, local), BF16),
            pltpu.VMEM((cache_len, local), BF16),
            pltpu.VMEM((local, keys), BF16),
            pltpu.VMEM((steps * span, local), BF16),
            pltpu.VMEM((steps * span, local), BF16),
            pltpu.VMEM(out_weight.shape, BF16),
            pltpu.VMEM((n, pairs, 2 * width, rows), BF16),
            pltpu.VMEM((all_heads, padded), F32),
            pltpu.VMEM((heads, 128), F32),
            pltpu.VMEM((heads, 128), F32),
            pltpu.VMEM((heads, rows), F32),
            pltpu.VMEM((keys, 128), BF16),
            pltpu.VMEM((pairs, 128, 2 * rows), BF16),
            pltpu.VMEM((n, pairs, 2 * width, rows), F32),
            pltpu.VMEM((n, pairs, 2, rows), F32),
            pltpu.VMEM((n, pairs, 2 * width, rows), BF16),
            pltpu.VMEM((n, pairs, 2 * width, rows), BF16),
            pltpu.VMEM((n, pairs, 2, rows), F32),
            pltpu.VMEM((n, pairs, 2, rows), F32),
            pltpu.VMEM((pairs, 2 * width, rows), F32),
            pltpu.VMEM((pairs, 2, rows), F32),
            pltpu.VMEM((2 * pairs, padded, 2 * width), BF16),
            dma((20,)),
            dma((n, pairs)), dma((n, pairs)), dma((n, pairs)),
            dma(()), dma(()),
            dma((2, n, pairs)), dma((2, n, pairs)), dma((2, n, pairs)), dma((2, n, pairs)),
            dma((pairs,)), dma((pairs,)),
        ],
        compiler_params=pltpu.CompilerParams(
            collective_id=0, has_side_effects=True, vmem_limit_bytes=60 * 1024 * 1024
        ),
    )(
        piece_tokens, step_tokens, norm_gain.reshape(1, -1), gate_weight.T,
        gate_bias.reshape(1, -1), decay_total.reshape(1, -1), cache_decay, step_gates,
        step_lengths, query_weight, key_weight, value_weight,
        cache_keys, cache_values,
        step_keys.reshape(steps * span, local), step_values.reshape(steps * span, local),
        out_weight,
    )


def solution(mesh):
    rows = P(("dp", "kv"), None)
    both = P(("dp", "kv"), "tp")
    cols = P(None, "tp")
    in_specs = (
        rows, rows, P(), cols, cols, cols, P(), P(), cols, both, both,
        P("tp", ("dp", "kv")), P("dp"),
        P(("dp", "kv"), None, "tp"), P(("dp", "kv"), None, "tp"),
        P(("dp", "kv"), "tp", None), P(("dp", "kv")),
    )
    return jax.shard_map(
        per_device, mesh=mesh, in_specs=in_specs, out_specs=(both, both), check_vma=False
    )
```

time: 39.1 us -> 39.4 us (level)
  Pallas kernels: 36.6 us -> 34.6 us
  local copies, waits for them, and re-layouts: 0.96 us -> 2.95 us
    pallas_call x2 -> x1, Pallas kernels: 36.6 us -> 34.6 us  [per_device(): pl.pallas_call(functools.partial(kernel, n, heads, width), out_shape=(jax...]
    unnamed x4 -> x2, local copies, waits for them, and re-layouts: 0.96 us -> 2.95 us
where the time goes in v1:
time: 39.4 us; the launch traced here: 38.9 us
  Pallas kernels  34.6 us (88%)
  local copies, waits for them, and re-layouts  2.95 us (7%)
  between operations  1.29 us (3%)
    pallas_call x1, Pallas kernels, per_device(): pl.pallas_call(functools.partial(kernel, n, heads, width), out_shape=(jax...  34.6 us
    unnamed x2, local copies, waits for them, and re-layouts  2.95 us

profile of v1, /device:TPU:0, one launch (start us, length us, event | category | flops | bytes accessed | tf_op | source)
XLA Modules:
  0.0 38.9 jit_solution(3694752539488376821)
XLA Ops:
  1.3 34.6 %shard_map.176 = (bf16[128,1024]{1,0:T(8,128)(2,1)}, bf16[1,1024]{1,0:T(2,128)(2,1)}) custom-call(bf16[128,2048]{1,0:T(8,128)(2,1)} %tok_h.1, bf16[1,2048]{1,0:T(2,128)(2,1)} %stok_h.1, f32[1,2048]{1,0:T(1,128)} %bitcast.9, bf16[16,2048]{1,0:T(8,128)(2,1)} %bitcast.8, f32[1,16]{1,0:T(1,128)} %bitcast.10, f32[1,16]{1,0:T(1,128)} %bitcast.11, ...), custom_call_target="tpu_custom_call" | custom-call | tf_op jit(solution)/shard_map/pallas_call | solution.py:577
  35.9 1.7 %copy.22 = bf16[128,1024]{1,0:T(8,128)(2,1)} copy(bf16[128,1024]{1,0:T(8,128)(2,1)} %get-tuple-element.4) | data formatting | bytes 524288
  37.6 1.3 %copy.23 = bf16[1,1024]{1,0:T(2,128)(2,1)} copy(bf16[1,1024]{1,0:T(2,128)(2,1)} %get-tuple-element.5) | data formatting | bytes 4096

commit v2 on v1

v2 whole, which is shorter than its diff:
```python
import functools
import math

import jax
import jax.numpy as jnp
from jax import lax
from jax.experimental import pallas as pl
from jax.experimental.pallas import tpu as pltpu
from jax.sharding import PartitionSpec as P

norm_eps = 1e-06
negative = -1e30
log2e = math.log2(math.e)
MESH = pl.DeviceIdType.MESH
F32 = jnp.float32
BF16 = jnp.bfloat16
NT = (((1,), (1,)), ((), ()))


def mark(name):
    return


def iota(shape, dim):
    return lax.broadcasted_iota(jnp.int32, shape, dim)


def normalize(rows, gain):
    wide = rows.astype(F32)
    factor = lax.rsqrt(jnp.mean(wide * wide, axis=-1, keepdims=True) + norm_eps)
    return (wide * factor * gain).astype(BF16)


def to_column(row, count):
    eye = iota((count, count), 0) == iota((count, count), 1)
    return jnp.sum(jnp.where(eye, row, 0.0), axis=1, keepdims=True)


def kernel(
    n, heads, width,
    tok_h, stok_h, gain_h, gate_w_h, gate_b_h, total_h, cache_decay_h, step_gates_h, step_len_h,
    wq, wk, wv, cache_k, cache_v, step_k, step_v,
    out_att,
    tok, stok, gain, gate_w, gate_b, total_decay, cache_decay, step_gates, step_len,
    nrm, wq_v, wk_v, wv_v, k_all, cv_v, v_turned, sk_v, sv_v,
    q_all, lg, gate_in, gate_out, bias_rows, bias_lanes, picks,
    own_mean, own_stat, to_r, to_l, stat_r, stat_l, near, near_stat, own_final, own_final_stat, att,
    local_sem, q_right, q_left, q_far, q_recv, g_send, g_recv, far_sem,
    m_send, m_recv, s_send, s_recv, x_send, x_recv,
):
    me = lax.axis_index("kv")
    tp = lax.axis_index("tp")
    rows = tok.shape[0]
    steps = stok.shape[0]
    cache_len = cache_k.shape[0]
    span = step_k.shape[0] // steps
    local = heads * width
    pair_lanes = 2 * width
    pairs = heads // 2
    keys = cache_len + rows
    root = math.sqrt(width)
    scale = log2e / root

    count = [0]

    def fetch(src, dst):
        copy = pltpu.make_async_copy(src, dst, local_sem.at[count[0]])
        count[0] += 1
        copy.start()
        return copy

    halves = 2 if local % 256 == 0 else 1
    part = local // halves
    c_tok = fetch(tok_h, tok)
    c_gain = fetch(gain_h, gain)
    c_stok = fetch(stok_h, stok)
    c_wq = [
        fetch(wq.at[:, pl.ds(c * part, part)], wq_v.at[:, pl.ds(c * part, part)])
        for c in range(halves)
    ]
    c_gw = fetch(gate_w_h, gate_w)
    c_gb = fetch(gate_b_h, gate_b)
    c_wk = fetch(wk, wk_v)
    c_wv = fetch(wv, wv_v)
    c_ck = fetch(cache_k, k_all.at[pl.ds(0, cache_len)])
    c_cv = fetch(cache_v, cv_v)
    c_td = fetch(total_h, total_decay)
    c_cd = fetch(cache_decay_h, cache_decay)
    c_sk = fetch(step_k, sk_v)
    c_sv = fetch(step_v, sv_v)
    c_sg = fetch(step_gates_h, step_gates)
    c_sl = fetch(step_len_h, step_len)

    has_right = me < n - 1
    has_left = me > 0
    right = lax.rem(me + 1, n)
    left = lax.rem(me + n - 1, n)

    reach = n >= 4
    first, last = 0, n - 1
    middle = jnp.logical_and(has_left, has_right)
    edge = jnp.logical_not(middle)

    def both(a, b):
        return jnp.logical_and(a, b)

    def as_count(flag):
        return flag.astype(jnp.int32)

    barrier = pltpu.get_barrier_semaphore()

    def hello(condition, target):
        @pl.when(condition)
        def _():
            pl.semaphore_signal(barrier, inc=1, device_id={"kv": target}, device_id_type=MESH)

    hello(has_right, right)
    hello(has_left, left)
    pl.semaphore_signal(barrier, inc=1, device_id={"tp": 1 - tp}, device_id_type=MESH)
    greeted = 1 + as_count(has_right) + as_count(has_left)
    if reach:
        hello(me == first, last)
        hello(me == first, 2)
        hello(me == n - 3, last)
        greeted = greeted + 2 * as_count(me == last) + as_count(me == 2)

    def enter():
        pl.semaphore_wait(barrier, greeted)
        if reach:
            @pl.when(me == last)
            def _():
                for target in (first, n - 3):
                    pl.semaphore_signal(
                        far_sem, inc=1, device_id={"kv": target}, device_id_type=MESH
                    )

    def q_copy(source, p, sem, target):
        return pltpu.make_async_remote_copy(
            src_ref=q_all.at[source, p], dst_ref=q_all.at[source, p],
            send_sem=sem, recv_sem=q_recv.at[source, p],
            device_id={"kv": target}, device_id_type=MESH,
        )

    def q_to_right(source, p):
        return q_copy(source, p, q_right.at[source], right)

    def q_to_left(source, p):
        return q_copy(source, p, q_left.at[source], left)

    def q_to_far(p):
        return q_copy(me, p, q_far, last - me)

    size = 2 if pairs % 2 == 0 else 1
    groups = [range(g, g + size) for g in range(0, pairs, size)]

    def part_target(side, owner):
        if side == 0:
            straight = both(owner == last, me == n - 3)
            return jnp.where(straight, last, right) if reach else right
        straight = both(owner == first, me == 2)
        return jnp.where(straight, first, left) if reach else left

    def part_slot(side, owner, target):
        return owner if side == 0 else jnp.where(owner == target, n, owner)

    def mean_copy(side, owner, p):
        means = to_r if side == 0 else to_l
        target = part_target(side, owner)
        return pltpu.make_async_remote_copy(
            src_ref=means.at[owner, p], dst_ref=means.at[owner, p],
            send_sem=m_send.at[owner], recv_sem=m_recv.at[part_slot(side, owner, target), p],
            device_id={"kv": target}, device_id_type=MESH,
        )

    def stat_copy(side, owner, g):
        stats = stat_r if side == 0 else stat_l
        target = part_target(side, owner)
        return pltpu.make_async_remote_copy(
            src_ref=stats.at[owner, g], dst_ref=stats.at[owner, g],
            send_sem=s_send.at[owner], recv_sem=s_recv.at[part_slot(side, owner, target), g],
            device_id={"kv": target}, device_id_type=MESH,
        )

    def near_mean(p):
        return pltpu.make_async_remote_copy(
            src_ref=near.at[p], dst_ref=near.at[p],
            send_sem=m_send.at[n], recv_sem=m_recv.at[n + 1, p],
            device_id={"kv": jnp.where(me == 1, first, last)}, device_id_type=MESH,
        )

    def near_level(g):
        return pltpu.make_async_remote_copy(
            src_ref=near_stat.at[g], dst_ref=near_stat.at[g],
            send_sem=s_send.at[n], recv_sem=s_recv.at[n + 1, g],
            device_id={"kv": jnp.where(me == 1, first, last)}, device_id_type=MESH,
        )

    def await_mean(means, slot, owner, p):
        pltpu.make_async_remote_copy(
            src_ref=means.at[owner, p], dst_ref=means.at[owner, p],
            send_sem=m_send.at[owner], recv_sem=m_recv.at[slot, p],
            device_id={"tp": 1 - tp}, device_id_type=MESH,
        ).wait_recv()

    def await_stat(stats, slot, owner, g):
        pltpu.make_async_remote_copy(
            src_ref=stats.at[owner, g], dst_ref=stats.at[owner, g],
            send_sem=s_send.at[owner], recv_sem=s_recv.at[slot, g],
            device_id={"tp": 1 - tp}, device_id_type=MESH,
        ).wait_recv()

    def all_sent(ref, sem, recv):
        pltpu.make_async_remote_copy(
            src_ref=ref, dst_ref=ref, send_sem=sem, recv_sem=recv,
            device_id={"tp": 1 - tp}, device_id_type=MESH,
        ).wait_send()

    @pl.when(me == last)
    def _():
        enter()

    mark("start")
    c_tok.wait()
    c_gain.wait()
    c_stok.wait()
    mark("tok")
    nrm[pl.ds(0, rows)] = normalize(tok[...], gain[...])
    pad = nrm.shape[0] - rows
    step_norm = normalize(stok[...], gain[...]).astype(F32)
    step_rows = jnp.zeros((pad, nrm.shape[1]), F32)
    for b in range(steps):
        step_rows = jnp.where(iota((pad, nrm.shape[1]), 0) == b, step_norm[b : b + 1], step_rows)
    nrm[pl.ds(rows, pad)] = step_rows.astype(BF16)

    mark("norm")
    def send_queries(which):
        for p in which:
            @pl.when(has_right)
            def _():
                q_to_right(me, p).start()

            @pl.when(has_left)
            def _():
                q_to_left(me, p).start()

    pairs_in_part = part // pair_lanes
    step_q_parts = []
    for c in range(halves):
        c_wq[c].wait()
        mark("wq")
        q_new = jnp.dot(
            nrm[...], wq_v[:, c * part : (c + 1) * part], preferred_element_type=F32
        ).astype(BF16)
        turned = q_new[:rows].T
        for i in range(pairs_in_part):
            q_all[me, c * pairs_in_part + i] = turned[i * pair_lanes : (i + 1) * pair_lanes]
        step_q_parts.append(q_new[rows:].astype(F32))

        @pl.when(has_left)
        def _():
            if c == 0:
                @pl.when(has_right)
                def _():
                    enter()

            send_queries(range(c * pairs_in_part, (c + 1) * pairs_in_part))

    @pl.when(jnp.logical_not(has_left))
    def _():
        enter()
        send_queries(range(pairs))

    if reach:
        @pl.when(me == last)
        def _():
            for p in range(pairs):
                q_to_far(p).start()

    step_q = jnp.concatenate(step_q_parts, axis=1)

    mark("qsent")
    c_gw.wait()
    c_gb.wait()
    logits = lax.dot_general(gate_w[...], nrm[...], NT, preferred_element_type=F32)
    logits = logits + to_column(gate_b[...], gate_w.shape[0])
    lg[...] = jnp.minimum(logits, 0.0) - jnp.log1p(jnp.exp(-jnp.abs(logits)))
    own_lg = lg[pl.ds(pl.multiple_of(tp * heads, heads), heads), :]
    piece_lg = own_lg[:, :rows]
    own_sum = jnp.broadcast_to(jnp.sum(piece_lg, axis=1, keepdims=True), gate_out.shape)

    g_copy = pltpu.make_async_remote_copy(
        src_ref=gate_out, dst_ref=gate_in, send_sem=g_send, recv_sem=g_recv,
        device_id={"kv": right}, device_id_type=MESH,
    )

    @pl.when(jnp.logical_not(has_left))
    def _():
        gate_in[...] = jnp.zeros(gate_in.shape, F32)
        gate_out[...] = own_sum

        @pl.when(has_right)
        def _():
            g_copy.start()

        if reach:
            pl.semaphore_wait(far_sem, 1)
            for p in range(pairs):
                q_to_far(p).start()

    mark("gates")
    c_wk.wait()
    c_wv.wait()
    c_cv.wait()
    c_td.wait()
    c_cd.wait()
    c_ck.wait()
    k_new = jnp.dot(nrm[...], wk_v[...], preferred_element_type=F32).astype(BF16)
    k_all[pl.ds(cache_len, rows)] = k_new[:rows]
    step_nk = k_new[rows:].astype(F32)
    v_new = jnp.dot(nrm[...], wv_v[...], preferred_element_type=F32).astype(BF16)
    v_turned[:, pl.ds(cache_len, rows)] = v_new[:rows].T
    step_nv = v_new[rows:].astype(F32)
    v_turned[:, pl.ds(0, cache_len)] = cv_v[...].T

    upto = (iota((rows, rows), 0) <= iota((rows, rows), 1)).astype(F32)
    running = jnp.dot(
        piece_lg, upto, preferred_element_type=F32, precision=lax.Precision.HIGHEST
    )

    def bias_terms(bias):
        high = bias.astype(BF16).astype(F32)
        rest = bias - high
        middle = rest.astype(BF16).astype(F32)
        low = rest - middle
        blank = jnp.zeros((128 - 3 * heads, bias.shape[1]), F32)
        return jnp.concatenate([high, middle, low, blank], axis=0).T.astype(BF16)

    lg_start = to_column(total_decay[...], gate_w.shape[0])
    start_rows = jnp.where(tp == 0, lg_start[:heads], lg_start[heads : 2 * heads])
    bias_lanes[pl.ds(0, cache_len)] = bias_terms((start_rows - cache_decay[...]) * root)
    bias_rows[...] = running

    head_of_column = lax.div(iota((128, 2 * rows), 1), rows)
    lane_of_term = iota((128, 2 * rows), 0)
    for p in range(pairs):
        hit = jnp.logical_and(
            lax.rem(lane_of_term, heads) == 2 * p + head_of_column, lane_of_term < 3 * heads
        )
        picks[p] = hit.astype(F32).astype(BF16)

    mark("bias")
    def finish_bias():
        @pl.when(has_left)
        def _():
            g_copy.wait_recv()

            @pl.when(has_right)
            def _():
                gate_out[...] = gate_in[...] + own_sum
                g_copy.start()

        fresh = -(gate_in[:, :1] + bias_rows[...]) * root
        bias_lanes[pl.ds(cache_len, rows)] = bias_terms(fresh)

    mark("fin")
    first_rows = iota((pair_lanes, rows), 0) < width
    causal = lax.rem(iota((rows, 2 * rows), 1), rows) >= iota((rows, 2 * rows), 0)

    def spread(two):
        return jnp.concatenate(
            [
                jnp.broadcast_to(two[0:1], (width, rows)),
                jnp.broadcast_to(two[1:2], (width, rows)),
            ],
            axis=0,
        )

    def scores_of(source, p, used):
        q_pair = q_all[source, p]
        zero = jnp.zeros_like(q_pair)
        rhs = jnp.concatenate(
            [
                jnp.concatenate(
                    [jnp.where(first_rows, q_pair, zero), jnp.where(first_rows, zero, q_pair)],
                    axis=1,
                ),
                picks[p],
            ],
            axis=0,
        )
        lanes = pl.ds(p * pair_lanes, pair_lanes)
        lhs = jnp.concatenate([k_all[pl.ds(0, used), lanes], bias_lanes[pl.ds(0, used)]], axis=1)
        return jnp.dot(lhs, rhs, preferred_element_type=F32)

    def weigh(raw):
        high = jnp.max(raw, axis=0, keepdims=True)
        weight = jnp.exp2((raw - high) * scale)
        mass = jnp.sum(weight, axis=0, keepdims=True)
        return weight.astype(BF16), mass, high * scale + jnp.log2(mass)

    def attend(source, group, used, masked):
        raws = [scores_of(source, p, used) for p in group]
        if masked:
            raws = [
                jnp.concatenate(
                    [raw[:cache_len], jnp.where(causal, raw[cache_len:], negative)], axis=0
                )
                for raw in raws
            ]
        weighed = [weigh(raw) for raw in raws]
        results = []
        for p, (weight, mass, level) in zip(group, weighed):
            values = v_turned[pl.ds(p * pair_lanes, pair_lanes), pl.ds(0, used)]
            mix = jnp.dot(values, weight, preferred_element_type=F32) * (1.0 / mass)
            mean = jnp.concatenate([mix[:width, :rows], mix[width:, rows:]], axis=0)
            levels = jnp.concatenate([level[:, :rows], level[:, rows:]], axis=0)
            results.append((p, mean, levels))
        return results

    def shares_of(levels):
        best = functools.reduce(jnp.maximum, levels)
        shares = [jnp.exp2(level - best) for level in levels]
        total = functools.reduce(jnp.add, shares)
        inverse = 1.0 / total
        return [share * inverse for share in shares], best + jnp.log2(total)

    def blend(shares, means, i):
        return functools.reduce(
            jnp.add,
            [spread(share[2 * i : 2 * i + 2]) * mean for share, mean in zip(shares, means)],
        )

    def stack(results):
        return jnp.concatenate([level for _, _, level in results], axis=0)

    def relay(from_left, k, group):
        if from_left:
            source, make, there, skip = me - k, q_to_right, me >= k, both(me - k == first, me == n - 2)
        else:
            source, make, there, skip = me + k, q_to_left, me + k < n, both(me + k == last, me == 1)

        @pl.when(there)
        def _():
            for p in group:
                make(source, p).wait_recv()
                if reach:
                    @pl.when(jnp.logical_not(skip))
                    def _():
                        make(source, p).start()
                else:
                    make(source, p).start()

    def keep(source, g, results):
        for p, mean, level in results:
            own_mean[source, p] = mean
        own_stat[source, g] = stack(results)

    def keep_near(g, results):
        for p, mean, level in results:
            near[p] = mean.astype(BF16)
        near_stat[g] = stack(results)
        near_level(g).start()
        for p, _, _ in results:
            near_mean(p).start()

    def attend_middle(from_left, k, g):
        source, used, there = (
            (me - k, cache_len, me >= k) if from_left else (me + k, keys, me + k < n)
        )
        relay(from_left, k, groups[g])

        @pl.when(there)
        def _():
            mark("L" if from_left else "R")
            results = attend(source, groups[g], used, False)
            if reach:
                is_near = (
                    both(source == first, k == 1) if from_left else both(source == last, k == 1)
                )

                @pl.when(is_near)
                def _():
                    keep_near(g, results)

                @pl.when(jnp.logical_not(is_near))
                def _():
                    keep(source, g, results)
            else:
                keep(source, g, results)

    def attend_edge(from_left, k, g):
        source, used, side = (me - k, cache_len, 1) if from_left else (me + k, keys, 0)
        means, stats = (to_l, stat_l) if from_left else (to_r, stat_r)
        make = q_to_right if from_left else q_to_left
        for p in groups[g]:
            make(source, p).wait_recv()
        mark("L" if from_left else "R")
        results = attend(source, groups[g], used, False)
        for p, mean, level in results:
            means[source, p] = mean.astype(BF16)
        stats[source, g] = stack(results)
        stat_copy(side, source, g).start()
        for p in groups[g]:
            mean_copy(side, source, p).start()

    def attend_own():
        mark("own")
        results = attend(me, range(pairs), keys, True)
        for p, mean, level in results:
            own_final[p] = mean
        for g, group in enumerate(groups):
            own_final_stat[g] = stack([results[p] for p in group])

    def decode():
        head_mask = lax.div(iota((heads, local), 1), width) == iota((heads, local), 0)
        chunk = 128
        chunks = span // chunk
        later = (iota((chunk, chunk), 0) > iota((chunk, chunk), 1)).astype(F32)
        c_sk.wait()
        c_sv.wait()
        c_sg.wait()
        c_sl.wait()
        step_att = jnp.zeros((pad, local), F32)
        for b in range(steps):
            length = step_len[0, b]
            in_cache = iota((heads, span), 1) < length
            kept = jnp.where(in_cache, step_gates[b], 0.0)
            tail = jnp.zeros((heads, 1), F32)
            parts = [None] * chunks
            for c in reversed(range(chunks)):
                piece = kept[:, c * chunk : (c + 1) * chunk]
                inner = jnp.dot(
                    piece, later, preferred_element_type=F32, precision=lax.Precision.HIGHEST
                )
                parts[c] = inner + tail
                tail = tail + jnp.sum(piece, axis=1, keepdims=True)
            after = jnp.concatenate(parts, axis=1)
            q_row = jnp.where(head_mask, step_q[b : b + 1], 0.0)
            scores = lax.dot_general(
                q_row.astype(BF16), sk_v[pl.ds(b * span, span)], NT, preferred_element_type=F32
            )
            new_lg = own_lg[:, rows + b : rows + b + 1]
            scores = scores * scale + (new_lg + after) * log2e
            scores = jnp.where(in_cache, scores, negative)
            self_score = jnp.sum(q_row * step_nk[b : b + 1], axis=1, keepdims=True) * scale
            high = jnp.maximum(jnp.max(scores, axis=1, keepdims=True), self_score)
            weight = jnp.exp2(scores - high)
            self_weight = jnp.exp2(self_score - high)
            mass = jnp.sum(weight, axis=1, keepdims=True) + self_weight
            mix = jnp.dot(
                weight.astype(BF16), sv_v[pl.ds(b * span, span)], preferred_element_type=F32
            )
            mix = mix + self_weight.astype(BF16).astype(F32) * step_nv[b : b + 1]
            one = jnp.sum(jnp.where(head_mask, mix / mass, 0.0), axis=0, keepdims=True)
            step_att = jnp.where(iota((pad, local), 0) == b, one, step_att)
        done = step_att.astype(BF16)
        for p in range(pairs):
            att[tp * pairs + p, pl.ds(rows, pad)] = done[:, p * pair_lanes : (p + 1) * pair_lanes]

    def in_order(i):
        return jnp.where(i == 1, 1, jnp.where(i == 2, n - 1, i - 1))

    @pl.when(jnp.logical_not(has_left))
    def _():
        finish_bias()

    @pl.when(edge)
    def _():
        def step(i, carry):
            k = in_order(i)
            for g in range(len(groups)):
                @pl.when(has_left)
                def _():
                    attend_edge(True, k, g)

                @pl.when(has_right)
                def _():
                    attend_edge(False, k, g)

            return carry

        lax.fori_loop(1, n, step, 0)

        @pl.when(has_left)
        def _():
            finish_bias()

        attend_own()
        mark("dec")
        decode()

    @pl.when(middle)
    def _():
        @pl.when(me == 1)
        def _():
            finish_bias()

        def step(k, carry):
            for g in range(len(groups)):
                attend_middle(True, k, g)

            @pl.when(both(k == 1, me > 1))
            def _():
                mark("bias")
                finish_bias()

            for g in range(len(groups)):
                attend_middle(False, k, g)

            @pl.when(k == 1)
            def _():
                attend_own()

            return carry

        lax.fori_loop(1, n, step, 0)
        mark("dec")
        decode()

    mark("loop")
    def forward(side, owner):
        means, stats = (to_r, stat_r) if side == 0 else (to_l, stat_l)
        for g, group in enumerate(groups):
            await_stat(stats, owner, owner, g)
            shares, level = shares_of([stats[owner, g], own_stat[owner, g]])
            stats[owner, g] = level
            stat_copy(side, owner, g).start()
            for i, p in enumerate(group):
                await_mean(means, owner, owner, p)
                mark("F")
                mean = blend(shares, [means[owner, p].astype(F32), own_mean[owner, p]], i)
                means[owner, p] = mean.astype(BF16)
                mean_copy(side, owner, p).start()

    def pass_right(r):
        due = both(has_left, r > me)
        if reach:
            due = both(due, jnp.logical_not(both(r == last, me == n - 2)))

        @pl.when(due)
        def _():
            if reach:
                @pl.when(both(r == last, me == n - 3))
                def _():
                    pl.semaphore_wait(far_sem, 1)

            forward(0, r)

    def pass_left(r):
        owner = n - 1 - r
        due = both(has_right, owner < me)
        if reach:
            due = both(due, jnp.logical_not(both(owner == first, me == 1)))

        @pl.when(due)
        def _():
            forward(1, owner)

    def turn(i, carry):
        r = jnp.where(i == 1, n - 1, i - 1)

        @pl.when(2 * me < n)
        def _():
            pass_right(r)
            pass_left(r)

        @pl.when(2 * me >= n)
        def _():
            pass_left(r)
            pass_right(r)

        return carry

    @pl.when(middle)
    def _():
        lax.fori_loop(1, n, turn, 0)

    def swap_copy(core, p):
        slot = core * pairs + p
        return pltpu.make_async_remote_copy(
            src_ref=att.at[slot], dst_ref=att.at[slot],
            send_sem=x_send, recv_sem=x_recv.at[p],
            device_id={"tp": 1 - tp}, device_id_type=MESH,
        )

    def finish(from_left, from_right, from_near):
        for g, group in enumerate(groups):
            levels = [own_final_stat[g]]
            if from_near:
                near_level(g).wait_recv()
                levels.append(near_stat[g])
            if from_left:
                await_stat(stat_r, me, me, g)
                levels.append(stat_r[me, g])
            if from_right:
                await_stat(stat_l, n, me, g)
                levels.append(stat_l[me, g])
            shares, _ = shares_of(levels)
            for i, p in enumerate(group):
                means = [own_final[p]]
                if from_near:
                    near_mean(p).wait_recv()
                    means.append(near[p].astype(F32))
                if from_left:
                    await_mean(to_r, me, me, p)
                    means.append(to_r[me, p].astype(F32))
                if from_right:
                    await_mean(to_l, n, me, p)
                    means.append(to_l[me, p].astype(F32))
                mark("fn")
                att[tp * pairs + p, pl.ds(0, rows)] = blend(shares, means, i).T.astype(BF16)
                swap_copy(tp, p).start()

    @pl.when(middle)
    def _():
        finish(True, True, False)

    @pl.when(both(has_left, jnp.logical_not(has_right)))
    def _():
        finish(True, False, reach)

    @pl.when(both(has_right, jnp.logical_not(has_left)))
    def _():
        finish(False, True, reach)

    mark("fin_sent")
    for p in range(pairs):
        swap_copy(1 - tp, p).wait_recv()
    mark("swapped")
    for i in range(2 * pairs):
        out_att[:, i * pair_lanes : (i + 1) * pair_lanes] = att[i]

    all_sent(att.at[pl.ds(tp * pairs, pairs)], x_send, x_recv.at[0])

    @pl.when(has_right)
    def _():
        g_copy.wait_send()

    if reach:
        @pl.when(edge)
        def _():
            all_sent(q_all.at[me], q_far, q_recv.at[me, 0])

        @pl.when(jnp.logical_or(me == 1, me == n - 2))
        def _():
            all_sent(near, m_send.at[n], m_recv.at[n, 0])
            all_sent(near_stat, s_send.at[n], s_recv.at[n, 0])

    def sent(owner, carry):
        right_sent = both(has_right, owner <= me)
        left_sent = both(has_left, owner >= me)
        part_right = both(has_right, owner > me)
        part_left = both(has_left, owner < me)
        if reach:
            right_sent = both(right_sent, jnp.logical_not(both(owner == first, me == n - 2)))
            left_sent = both(left_sent, jnp.logical_not(both(owner == last, me == 1)))
            part_right = both(part_right, jnp.logical_not(both(owner == last, me == n - 2)))
            part_left = both(part_left, jnp.logical_not(both(owner == first, me == 1)))

        @pl.when(right_sent)
        def _():
            all_sent(q_all.at[owner], q_right.at[owner], q_recv.at[owner, 0])

        @pl.when(left_sent)
        def _():
            all_sent(q_all.at[owner], q_left.at[owner], q_recv.at[owner, 0])

        @pl.when(part_right)
        def _():
            all_sent(to_r.at[owner], m_send.at[owner], m_recv.at[owner, 0])
            all_sent(stat_r.at[owner], s_send.at[owner], s_recv.at[owner, 0])

        @pl.when(part_left)
        def _():
            all_sent(to_l.at[owner], m_send.at[owner], m_recv.at[owner, 0])
            all_sent(stat_l.at[owner], s_send.at[owner], s_recv.at[owner, 0])

        return carry

    lax.fori_loop(0, n, sent, 0)
    mark("sent")


def project(rows, att, weight, out_piece, out_step):
    projected = jnp.dot(att[...], weight[...], preferred_element_type=F32)
    out_piece[...] = projected[:rows].astype(BF16)
    out_step[...] = projected[rows : rows + out_step.shape[0]].astype(BF16)


def per_device(
    piece_tokens, step_tokens, norm_gain, query_weight, key_weight, value_weight,
    gate_weight, gate_bias, out_weight, cache_keys, cache_values, cache_decay,
    decay_total, step_keys, step_values, step_gates, step_lengths,
):
    n = lax.axis_size("kv")
    rows, model = piece_tokens.shape
    steps = step_tokens.shape[0]
    heads = cache_decay.shape[0]
    local = query_weight.shape[1]
    width = local // heads
    pairs = heads // 2
    groups = pairs // 2 if pairs % 2 == 0 else pairs
    cache_len = cache_keys.shape[0]
    keys = cache_len + rows
    span = step_keys.shape[1]
    columns = out_weight.shape[1]
    padded = rows + 16 * (-(-steps // 16))
    all_heads = gate_weight.shape[1]
    vmem = pl.BlockSpec(memory_space=pltpu.VMEM)
    hbm = pl.BlockSpec(memory_space=pltpu.HBM)
    dma = pltpu.SemaphoreType.DMA
    att = pl.pallas_call(
        functools.partial(kernel, n, heads, width),
        out_shape=pltpu.VMEM((padded, out_weight.shape[0]), BF16),
        in_specs=[hbm] * 16,
        out_specs=vmem,
        scratch_shapes=[
            pltpu.VMEM((rows, model), BF16),
            pltpu.VMEM((steps, model), BF16),
            pltpu.VMEM((1, model), F32),
            pltpu.VMEM((all_heads, model), BF16),
            pltpu.VMEM((1, all_heads), F32),
            pltpu.VMEM((1, all_heads), F32),
            pltpu.VMEM(cache_decay.shape, F32),
            pltpu.VMEM(step_gates.shape, F32),
            pltpu.SMEM((1, steps), jnp.int32),
            pltpu.VMEM((padded, model), BF16),
            pltpu.VMEM(query_weight.shape, BF16),
            pltpu.VMEM(key_weight.shape, BF16),
            pltpu.VMEM(value_weight.shape, BF16),
            pltpu.VMEM((keys, local), BF16),
            pltpu.VMEM((cache_len, local), BF16),
            pltpu.VMEM((local, keys), BF16),
            pltpu.VMEM((steps * span, local), BF16),
            pltpu.VMEM((steps * span, local), BF16),
            pltpu.VMEM((n, pairs, 2 * width, rows), BF16),
            pltpu.VMEM((all_heads, padded), F32),
            pltpu.VMEM((heads, 128), F32),
            pltpu.VMEM((heads, 128), F32),
            pltpu.VMEM((heads, rows), F32),
            pltpu.VMEM((keys, 128), BF16),
            pltpu.VMEM((pairs, 128, 2 * rows), BF16),
            pltpu.VMEM((n, pairs, 2 * width, rows), F32),
            pltpu.VMEM((n, groups, heads // groups, rows), F32),
            pltpu.VMEM((n, pairs, 2 * width, rows), BF16),
            pltpu.VMEM((n, pairs, 2 * width, rows), BF16),
            pltpu.VMEM((n, groups, heads // groups, rows), F32),
            pltpu.VMEM((n, groups, heads // groups, rows), F32),
            pltpu.VMEM((pairs, 2 * width, rows), BF16),
            pltpu.VMEM((groups, heads // groups, rows), F32),
            pltpu.VMEM((pairs, 2 * width, rows), F32),
            pltpu.VMEM((groups, heads // groups, rows), F32),
            pltpu.VMEM((2 * pairs, padded, 2 * width), BF16),
            dma((17,)),
            dma((n,)), dma((n,)), dma(()), dma((n, pairs)),
            dma(()), dma(()), pltpu.SemaphoreType.REGULAR,
            dma((n + 1,)), dma((n + 2, pairs)), dma((n + 1,)), dma((n + 2, groups)),
            dma(()), dma((pairs,)),
        ],
        compiler_params=pltpu.CompilerParams(
            collective_id=0, has_side_effects=True, vmem_limit_bytes=56 * 1024 * 1024
        ),
    )(
        piece_tokens, step_tokens, norm_gain.reshape(1, -1), gate_weight.T,
        gate_bias.reshape(1, -1), decay_total.reshape(1, -1), cache_decay, step_gates,
        step_lengths.reshape(1, -1), query_weight, key_weight, value_weight,
        cache_keys, cache_values,
        step_keys.reshape(steps * span, local), step_values.reshape(steps * span, local),
    )
    return pl.pallas_call(
        functools.partial(project, rows),
        out_shape=(
            jax.ShapeDtypeStruct((rows, columns), BF16),
            jax.ShapeDtypeStruct((steps, columns), BF16),
        ),
        in_specs=[vmem, vmem],
        out_specs=(vmem, vmem),
        compiler_params=pltpu.CompilerParams(vmem_limit_bytes=16 * 1024 * 1024),
    )(att, out_weight)


def solution(mesh):
    rows = P(("dp", "kv"), None)
    both = P(("dp", "kv"), "tp")
    cols = P(None, "tp")
    in_specs = (
        rows, rows, P(), cols, cols, cols, P(), P(), cols, both, both,
        P("tp", ("dp", "kv")), P("dp"),
        P(("dp", "kv"), None, "tp"), P(("dp", "kv"), None, "tp"),
        P(("dp", "kv"), "tp", None), P(("dp", "kv")),
    )
    return jax.shard_map(
        per_device, mesh=mesh, in_specs=in_specs, out_specs=(both, both), check_vma=False
    )
```

time: 39.4 us -> 29.4 us (0.75)
  the two profiles are of different devices: /device:TPU:0 before, /device:TPU:21 now
where the time goes in v2:
time: 29.4 us; the launch traced here: 29.2 us
  Pallas kernels  27.9 us (95%)
  between operations  1.31 us (4%)
    pallas_call x1, Pallas kernels, per_device(): pl.pallas_call(functools.partial(kernel, n, heads, width), out_shape=pltp...  26.7 us
    pallas_call x1, Pallas kernels, per_device(): pl.pallas_call(functools.partial(project, rows), out_shape=(jax.ShapeDtyp...  1.2 us

profile of v2, /device:TPU:21, one launch (start us, length us, event | category | flops | bytes accessed | tf_op | source)
XLA Modules:
  0.0 29.2 jit_solution(1101673061215860360)
XLA Ops:
  1.3 0.0 copy-start
  1.3 26.7 %shard_map.176.att = bf16[144,1024]{1,0:T(8,128)(2,1)S(1)} custom-call(bf16[128,2048]{1,0:T(8,128)(2,1)} %tok_h.1, bf16[1,2048]{1,0:T(2,128)(2,1)} %stok_h.1, f32[1,2048]{1,0:T(1,128)} %bitcast.11, bf16[16,2048]{1,0:T(8,128)(2,1)} %bitcast.10, f32[1,16]{1,0:T(1,128)} %bitcast.12, f32[1,16]{1,0:T(1,128)} %bitcast.13, f32[8,512]{1,0:T(8,128)} %cache_decay_h.1, ...), custom_call_target="tpu_custom_call" | custom-call | tf_op jit(solution)/shard_map/pallas_call | solution.py:812
  28.0 0.0 copy-done
  28.0 1.2 %shard_map.177 = (bf16[128,1024]{1,0:T(8,128)(2,1)}, bf16[1,1024]{1,0:T(2,128)(2,1)}) custom-call(bf16[144,1024]{1,0:T(8,128)(2,1)S(1)} %shard_map.176.att, bf16[1024,1024]{1,0:T(8,128)(2,1)S(1)} %copy-done), custom_call_target="tpu_custom_call" | custom-call | tf_op jit(solution)/shard_map/pallas_call | solution.py:870
Async XLA Ops:
  1.3 26.7 %copy-start = (bf16[1024,1024]{1,0:T(8,128)(2,1)S(1)}, bf16[1024,1024]{1,0:T(8,128)(2,1)}, u32[]{:S(2)}) copy-start(bf16[1024,1024]{1,0:T(8,128)(2,1)} %weight.1) | copy-start | bytes 6291460

commit v3 on v2

--- a/solution.py
+++ b/solution.py
@@ -17,8 +17,8 @@
 NT = (((1,), (1,)), ((), ()))
 
 
-def mark(name):
-    return
+def fence():
+    pl.delay(1)
 
 
 def iota(shape, dim):
@@ -78,25 +78,13 @@
         fetch(wq.at[:, pl.ds(c * part, part)], wq_v.at[:, pl.ds(c * part, part)])
         for c in range(halves)
     ]
-    c_gw = fetch(gate_w_h, gate_w)
-    c_gb = fetch(gate_b_h, gate_b)
-    c_wk = fetch(wk, wk_v)
-    c_wv = fetch(wv, wv_v)
-    c_ck = fetch(cache_k, k_all.at[pl.ds(0, cache_len)])
-    c_cv = fetch(cache_v, cv_v)
-    c_td = fetch(total_h, total_decay)
-    c_cd = fetch(cache_decay_h, cache_decay)
-    c_sk = fetch(step_k, sk_v)
-    c_sv = fetch(step_v, sv_v)
-    c_sg = fetch(step_gates_h, step_gates)
-    c_sl = fetch(step_len_h, step_len)
 
     has_right = me < n - 1
     has_left = me > 0
     right = lax.rem(me + 1, n)
     left = lax.rem(me + n - 1, n)
 
-    reach = n >= 4
+    reach = n == 4
     first, last = 0, n - 1
     middle = jnp.logical_and(has_left, has_right)
     edge = jnp.logical_not(middle)
@@ -119,20 +107,18 @@
     pl.semaphore_signal(barrier, inc=1, device_id={"tp": 1 - tp}, device_id_type=MESH)
     greeted = 1 + as_count(has_right) + as_count(has_left)
     if reach:
-        hello(me == first, last)
         hello(me == first, 2)
+        hello(me == 2, first)
         hello(me == n - 3, last)
-        greeted = greeted + 2 * as_count(me == last) + as_count(me == 2)
+        for each in (first, 2, last):
+            greeted = greeted + as_count(me == each)
 
     def enter():
         pl.semaphore_wait(barrier, greeted)
         if reach:
             @pl.when(me == last)
             def _():
-                for target in (first, n - 3):
-                    pl.semaphore_signal(
-                        far_sem, inc=1, device_id={"kv": target}, device_id_type=MESH
-                    )
+                pl.semaphore_signal(far_sem, inc=1, device_id={"kv": n - 3}, device_id_type=MESH)
 
     def q_copy(source, p, sem, target):
         return pltpu.make_async_remote_copy(
@@ -148,7 +134,7 @@
         return q_copy(source, p, q_left.at[source], left)
 
     def q_to_far(p):
-        return q_copy(me, p, q_far, last - me)
+        return q_copy(me, p, q_far, jnp.where(me == first, 2, n - 3))
 
     size = 2 if pairs % 2 == 0 else 1
     groups = [range(g, g + size) for g in range(0, pairs, size)]
@@ -215,15 +201,21 @@
             device_id={"tp": 1 - tp}, device_id_type=MESH,
         ).wait_send()
 
-    @pl.when(me == last)
-    def _():
-        enter()
-
-    mark("start")
     c_tok.wait()
     c_gain.wait()
     c_stok.wait()
-    mark("tok")
+    c_gw = fetch(gate_w_h, gate_w)
+    c_gb = fetch(gate_b_h, gate_b)
+    c_wk = fetch(wk, wk_v)
+    c_wv = fetch(wv, wv_v)
+    c_cv = fetch(cache_v, cv_v)
+    c_ck = fetch(cache_k, k_all.at[pl.ds(0, cache_len)])
+    c_td = fetch(total_h, total_decay)
+    c_cd = fetch(cache_decay_h, cache_decay)
+    c_sk = fetch(step_k, sk_v)
+    c_sv = fetch(step_v, sv_v)
+    c_sg = fetch(step_gates_h, step_gates)
+    c_sl = fetch(step_len_h, step_len)
     nrm[pl.ds(0, rows)] = normalize(tok[...], gain[...])
     pad = nrm.shape[0] - rows
     step_norm = normalize(stok[...], gain[...]).astype(F32)
@@ -232,7 +224,6 @@
         step_rows = jnp.where(iota((pad, nrm.shape[1]), 0) == b, step_norm[b : b + 1], step_rows)
     nrm[pl.ds(rows, pad)] = step_rows.astype(BF16)
 
-    mark("norm")
     def send_queries(which):
         for p in which:
             @pl.when(has_right)
@@ -247,7 +238,6 @@
     step_q_parts = []
     for c in range(halves):
         c_wq[c].wait()
-        mark("wq")
         q_new = jnp.dot(
             nrm[...], wq_v[:, c * part : (c + 1) * part], preferred_element_type=F32
         ).astype(BF16)
@@ -256,29 +246,31 @@
             q_all[me, c * pairs_in_part + i] = turned[i * pair_lanes : (i + 1) * pair_lanes]
         step_q_parts.append(q_new[rows:].astype(F32))
 
+        chunk = range(c * pairs_in_part, (c + 1) * pairs_in_part)
+
         @pl.when(has_left)
         def _():
             if c == 0:
+                enter()
+            if reach:
                 @pl.when(has_right)
                 def _():
-                    enter()
-
-            send_queries(range(c * pairs_in_part, (c + 1) * pairs_in_part))
-
-    @pl.when(jnp.logical_not(has_left))
-    def _():
-        enter()
-        send_queries(range(pairs))
+                    send_queries(chunk)
+
+                @pl.when(jnp.logical_not(has_right))
+                def _():
+                    for p in chunk:
+                        q_to_far(p).start()
+            else:
+                send_queries(chunk)
 
     if reach:
-        @pl.when(me == last)
-        def _():
-            for p in range(pairs):
-                q_to_far(p).start()
+        @pl.when(jnp.logical_not(has_right))
+        def _():
+            send_queries(range(pairs))
 
     step_q = jnp.concatenate(step_q_parts, axis=1)
 
-    mark("qsent")
     c_gw.wait()
     c_gb.wait()
     logits = lax.dot_general(gate_w[...], nrm[...], NT, preferred_element_type=F32)
@@ -298,16 +290,17 @@
         gate_in[...] = jnp.zeros(gate_in.shape, F32)
         gate_out[...] = own_sum
 
+        enter()
+
         @pl.when(has_right)
         def _():
             g_copy.start()
 
         if reach:
-            pl.semaphore_wait(far_sem, 1)
             for p in range(pairs):
                 q_to_far(p).start()
-
-    mark("gates")
+        send_queries(range(pairs))
+
     c_wk.wait()
     c_wv.wait()
     c_cv.wait()
@@ -348,8 +341,7 @@
         )
         picks[p] = hit.astype(F32).astype(BF16)
 
-    mark("bias")
-    def finish_bias():
+    def pass_prefix():
         @pl.when(has_left)
         def _():
             g_copy.wait_recv()
@@ -359,10 +351,10 @@
                 gate_out[...] = gate_in[...] + own_sum
                 g_copy.start()
 
+    def finish_bias():
         fresh = -(gate_in[:, :1] + bias_rows[...]) * root
         bias_lanes[pl.ds(cache_len, rows)] = bias_terms(fresh)
 
-    mark("fin")
     first_rows = iota((pair_lanes, rows), 0) < width
     causal = lax.rem(iota((rows, 2 * rows), 1), rows) >= iota((rows, 2 * rows), 0)
 
@@ -388,9 +380,11 @@
             ],
             axis=0,
         )
-        lanes = pl.ds(p * pair_lanes, pair_lanes)
-        lhs = jnp.concatenate([k_all[pl.ds(0, used), lanes], bias_lanes[pl.ds(0, used)]], axis=1)
+        lhs = jnp.concatenate([k_all[pl.ds(0, used), lanes_of(p)], bias_lanes[pl.ds(0, used)]], axis=1)
         return jnp.dot(lhs, rhs, preferred_element_type=F32)
+
+    def lanes_of(p):
+        return pl.ds(pl.multiple_of(p * pair_lanes, pair_lanes), pair_lanes)
 
     def weigh(raw):
         high = jnp.max(raw, axis=0, keepdims=True)
@@ -410,7 +404,7 @@
         weighed = [weigh(raw) for raw in raws]
         results = []
         for p, (weight, mass, level) in zip(group, weighed):
-            values = v_turned[pl.ds(p * pair_lanes, pair_lanes), pl.ds(0, used)]
+            values = v_turned[lanes_of(p), pl.ds(0, used)]
             mix = jnp.dot(values, weight, preferred_element_type=F32) * (1.0 / mass)
             mean = jnp.concatenate([mix[:width, :rows], mix[width:, rows:]], axis=0)
             levels = jnp.concatenate([level[:, :rows], level[:, rows:]], axis=0)
@@ -433,29 +427,35 @@
     def stack(results):
         return jnp.concatenate([level for _, _, level in results], axis=0)
 
-    def relay(from_left, k, group):
-        if from_left:
-            source, make, there, skip = me - k, q_to_right, me >= k, both(me - k == first, me == n - 2)
-        else:
-            source, make, there, skip = me + k, q_to_left, me + k < n, both(me + k == last, me == 1)
-
-        @pl.when(there)
-        def _():
-            for p in group:
-                make(source, p).wait_recv()
-                if reach:
-                    @pl.when(jnp.logical_not(skip))
-                    def _():
-                        make(source, p).start()
-                else:
-                    make(source, p).start()
-
-    def keep(source, g, results):
+    def in_group(g):
+        return [g * size + i for i in range(size)]
+
+    def arrived(from_left, k, g):
+        for p in in_group(g):
+            if from_left:
+                q_to_right(me - k, p).wait_recv()
+            else:
+                q_to_left(me + k, p).wait_recv()
+
+    def relay(from_left, k, g):
+        for p in in_group(g):
+            if from_left:
+                q_to_right(me - k, p).start()
+            else:
+                q_to_left(me + k, p).start()
+
+    def attend_keep(from_left, k, g):
+        source, used = (me - k, cache_len) if from_left else (me + k, keys)
+        fence()
+        results = attend(source, in_group(g), used, False)
         for p, mean, level in results:
             own_mean[source, p] = mean
         own_stat[source, g] = stack(results)
 
-    def keep_near(g, results):
+    def attend_near(from_left, g):
+        source, used = (me - 1, cache_len) if from_left else (me + 1, keys)
+        fence()
+        results = attend(source, in_group(g), used, False)
         for p, mean, level in results:
             near[p] = mean.astype(BF16)
         near_stat[g] = stack(results)
@@ -463,48 +463,21 @@
         for p, _, _ in results:
             near_mean(p).start()
 
-    def attend_middle(from_left, k, g):
-        source, used, there = (
-            (me - k, cache_len, me >= k) if from_left else (me + k, keys, me + k < n)
-        )
-        relay(from_left, k, groups[g])
-
-        @pl.when(there)
-        def _():
-            mark("L" if from_left else "R")
-            results = attend(source, groups[g], used, False)
-            if reach:
-                is_near = (
-                    both(source == first, k == 1) if from_left else both(source == last, k == 1)
-                )
-
-                @pl.when(is_near)
-                def _():
-                    keep_near(g, results)
-
-                @pl.when(jnp.logical_not(is_near))
-                def _():
-                    keep(source, g, results)
-            else:
-                keep(source, g, results)
-
     def attend_edge(from_left, k, g):
         source, used, side = (me - k, cache_len, 1) if from_left else (me + k, keys, 0)
         means, stats = (to_l, stat_l) if from_left else (to_r, stat_r)
-        make = q_to_right if from_left else q_to_left
-        for p in groups[g]:
-            make(source, p).wait_recv()
-        mark("L" if from_left else "R")
-        results = attend(source, groups[g], used, False)
+        arrived(from_left, k, g)
+        fence()
+        results = attend(source, in_group(g), used, False)
         for p, mean, level in results:
             means[source, p] = mean.astype(BF16)
         stats[source, g] = stack(results)
         stat_copy(side, source, g).start()
-        for p in groups[g]:
+        for p in in_group(g):
             mean_copy(side, source, p).start()
 
     def attend_own():
-        mark("own")
+        fence()
         results = attend(me, range(pairs), keys, True)
         for p, mean, level in results:
             own_final[p] = mean
@@ -557,67 +530,132 @@
         for p in range(pairs):
             att[tp * pairs + p, pl.ds(rows, pad)] = done[:, p * pair_lanes : (p + 1) * pair_lanes]
 
-    def in_order(i):
-        return jnp.where(i == 1, 1, jnp.where(i == 2, n - 1, i - 1))
+    parts = len(groups)
+
+    def each_group(make):
+        def body(g, carry):
+            make(g)
+            return carry
+
+        lax.fori_loop(0, parts, body, 0)
 
     @pl.when(jnp.logical_not(has_left))
     def _():
+        pass_prefix()
         finish_bias()
 
     @pl.when(edge)
     def _():
         def step(i, carry):
-            k = in_order(i)
-            for g in range(len(groups)):
+            k = jnp.where(i == 1, 1, jnp.where(i == 2, n - 1, i - 1)) if reach else i
+
+            @pl.when(has_left)
+            def _():
+                each_group(lambda g: attend_edge(True, k, g))
+
+            @pl.when(has_right)
+            def _():
+                each_group(lambda g: attend_edge(False, k, g))
+
+            @pl.when(i == 1)
+            def _():
+                fence()
+                decode()
+
+            @pl.when(i == max(1, n - 2))
+            def _():
                 @pl.when(has_left)
                 def _():
-                    attend_edge(True, k, g)
-
-                @pl.when(has_right)
-                def _():
-                    attend_edge(False, k, g)
+                    pass_prefix()
+                    finish_bias()
+
+                attend_own()
 
             return carry
 
         lax.fori_loop(1, n, step, 0)
 
-        @pl.when(has_left)
-        def _():
+    if reach:
+        @pl.when(me == n - 3)
+        def _():
+            pass_prefix()
             finish_bias()
 
-        attend_own()
-        mark("dec")
-        decode()
+            def turn_one(i, carry):
+                k = 2 - i
+
+                def body(g):
+                    arrived(False, k, g)
+                    relay(False, k, g)
+                    attend_keep(False, k, g)
+
+                each_group(body)
+                return carry
+
+            lax.fori_loop(0, 2, turn_one, 0)
+
+            def body(g):
+                arrived(True, 1, g)
+                attend_near(True, g)
+
+            each_group(body)
+
+        @pl.when(me == 2)
+        def _():
+            def turn_two(i, carry):
+                k = 2 - i
+
+                def body(g):
+                    arrived(True, k, g)
+                    relay(True, k, g)
+                    attend_keep(True, k, g)
+
+                    @pl.when(both(i == 0, g == 0))
+                    def _():
+                        pass_prefix()
+
+                each_group(body)
+                return carry
+
+            lax.fori_loop(0, 2, turn_two, 0)
+            finish_bias()
+
+            def body(g):
+                arrived(False, 1, g)
+                attend_near(False, g)
+
+            each_group(body)
+    else:
+        @pl.when(middle)
+        def _():
+            pass_prefix()
+            finish_bias()
+
+            def step(k, carry):
+                for from_left, there in ((True, me >= k), (False, me + k < n)):
+                    @pl.when(there)
+                    def _():
+                        def body(g):
+                            arrived(from_left, k, g)
+                            relay(from_left, k, g)
+
+                        each_group(body)
+
+                for from_left, there in ((True, me >= k), (False, me + k < n)):
+                    @pl.when(there)
+                    def _():
+                        each_group(lambda g: attend_keep(from_left, k, g))
+
+                return carry
+
+            lax.fori_loop(1, n, step, 0)
 
     @pl.when(middle)
     def _():
-        @pl.when(me == 1)
-        def _():
-            finish_bias()
-
-        def step(k, carry):
-            for g in range(len(groups)):
-                attend_middle(True, k, g)
-
-            @pl.when(both(k == 1, me > 1))
-            def _():
-                mark("bias")
-                finish_bias()
-
-            for g in range(len(groups)):
-                attend_middle(False, k, g)
-
-            @pl.when(k == 1)
-            def _():
-                attend_own()
-
-            return carry
-
-        lax.fori_loop(1, n, step, 0)
-        mark("dec")
+        attend_own()
+        fence()
         decode()
 
-    mark("loop")
     def forward(side, owner):
         means, stats = (to_r, stat_r) if side == 0 else (to_l, stat_l)
         for g, group in enumerate(groups):
@@ -627,53 +665,48 @@
             stat_copy(side, owner, g).start()
             for i, p in enumerate(group):
                 await_mean(means, owner, owner, p)
-                mark("F")
                 mean = blend(shares, [means[owner, p].astype(F32), own_mean[owner, p]], i)
                 means[owner, p] = mean.astype(BF16)
                 mean_copy(side, owner, p).start()
 
-    def pass_right(r):
-        due = both(has_left, r > me)
-        if reach:
-            due = both(due, jnp.logical_not(both(r == last, me == n - 2)))
-
-        @pl.when(due)
-        def _():
-            if reach:
-                @pl.when(both(r == last, me == n - 3))
-                def _():
-                    pl.semaphore_wait(far_sem, 1)
-
-            forward(0, r)
-
-    def pass_left(r):
-        owner = n - 1 - r
-        due = both(has_right, owner < me)
-        if reach:
-            due = both(due, jnp.logical_not(both(owner == first, me == 1)))
-
-        @pl.when(due)
-        def _():
-            forward(1, owner)
-
-    def turn(i, carry):
-        r = jnp.where(i == 1, n - 1, i - 1)
-
-        @pl.when(2 * me < n)
-        def _():
-            pass_right(r)
-            pass_left(r)
-
-        @pl.when(2 * me >= n)
-        def _():
-            pass_left(r)
-            pass_right(r)
-
-        return carry
-
-    @pl.when(middle)
-    def _():
-        lax.fori_loop(1, n, turn, 0)
+    if reach:
+        @pl.when(me == n - 3)
+        def _():
+            pl.semaphore_wait(far_sem, 1)
+            forward(0, last)
+            forward(0, 2)
+
+        @pl.when(me == 2)
+        def _():
+            forward(1, first)
+            forward(1, n - 3)
+    else:
+        def pass_right(r):
+            @pl.when(both(has_left, r > me))
+            def _():
+                forward(0, r)
+
+        def pass_left(r):
+            @pl.when(both(has_right, n - 1 - r < me))
+            def _():
+                forward(1, n - 1 - r)
+
+        def turn(r, carry):
+            @pl.when(2 * me < n)
+            def _():
+                pass_right(r)
+                pass_left(r)
+
+            @pl.when(2 * me >= n)
+            def _():
+                pass_left(r)
+                pass_right(r)
+
+            return carry
+
+        @pl.when(middle)
+        def _():
+            lax.fori_loop(1, n, turn, 0)
 
     def swap_copy(core, p):
         slot = core * pairs + p
@@ -707,7 +740,6 @@
                 if from_right:
                     await_mean(to_l, n, me, p)
                     means.append(to_l[me, p].astype(F32))
-                mark("fn")
                 att[tp * pairs + p, pl.ds(0, rows)] = blend(shares, means, i).T.astype(BF16)
                 swap_copy(tp, p).start()
 
@@ -723,10 +755,8 @@
     def _():
         finish(False, True, reach)
 
-    mark("fin_sent")
     for p in range(pairs):
         swap_copy(1 - tp, p).wait_recv()
-    mark("swapped")
     for i in range(2 * pairs):
         out_att[:, i * pair_lanes : (i + 1) * pair_lanes] = att[i]
 
@@ -752,8 +782,8 @@
         part_right = both(has_right, owner > me)
         part_left = both(has_left, owner < me)
         if reach:
-            right_sent = both(right_sent, jnp.logical_not(both(owner == first, me == n - 2)))
-            left_sent = both(left_sent, jnp.logical_not(both(owner == last, me == 1)))
+            right_sent = both(right_sent, jnp.logical_not(both(owner == first, me == 1)))
+            left_sent = both(left_sent, jnp.logical_not(both(owner == last, me == n - 2)))
             part_right = both(part_right, jnp.logical_not(both(owner == last, me == n - 2)))
             part_left = both(part_left, jnp.logical_not(both(owner == first, me == 1)))
 
@@ -778,7 +808,6 @@
         return carry
 
     lax.fori_loop(0, n, sent, 0)
-    mark("sent")
 
 
 def project(rows, att, weight, out_piece, out_step):

time: 29.4 us -> 28.4 us (0.966)
  the two profiles are of different devices: /device:TPU:21 before, /device:TPU:0 now
where the time goes in v3:
time: 28.4 us; the launch traced here: 28.3 us
  Pallas kernels  27 us (95%)
  between operations  1.31 us (5%)
    pallas_call x1, Pallas kernels, per_device(): pl.pallas_call(functools.partial(kernel, n, heads, width), out_shape=pltp...  25.8 us
    pallas_call x1, Pallas kernels, per_device(): pl.pallas_call(functools.partial(project, rows), out_shape=(jax.ShapeDtyp...  1.2 us

profile of v3, /device:TPU:0, one launch (start us, length us, event | category | flops | bytes accessed | tf_op | source)
XLA Modules:
  0.0 28.3 jit_solution(8673558820961135674)
XLA Ops:
  1.3 0.0 copy-start
  1.3 25.8 %shard_map.176.att = bf16[144,1024]{1,0:T(8,128)(2,1)S(1)} custom-call(bf16[128,2048]{1,0:T(8,128)(2,1)} %tok_h.1, bf16[1,2048]{1,0:T(2,128)(2,1)} %stok_h.1, f32[1,2048]{1,0:T(1,128)} %bitcast.11, bf16[16,2048]{1,0:T(8,128)(2,1)} %bitcast.10, f32[1,16]{1,0:T(1,128)} %bitcast.12, f32[1,16]{1,0:T(1,128)} %bitcast.13, f32[8,512]{1,0:T(8,128)} %cache_decay_h.1, ...), custom_call_target="tpu_custom_call" | custom-call | tf_op jit(solution)/shard_map/pallas_call | solution.py:841
  27.1 0.0 copy-done
  27.1 1.2 %shard_map.177 = (bf16[128,1024]{1,0:T(8,128)(2,1)}, bf16[1,1024]{1,0:T(2,128)(2,1)}) custom-call(bf16[144,1024]{1,0:T(8,128)(2,1)S(1)} %shard_map.176.att, bf16[1024,1024]{1,0:T(8,128)(2,1)S(1)} %copy-done), custom_call_target="tpu_custom_call" | custom-call | tf_op jit(solution)/shard_map/pallas_call | solution.py:899
Async XLA Ops:
  1.3 25.8 %copy-start = (bf16[1024,1024]{1,0:T(8,128)(2,1)S(1)}, bf16[1024,1024]{1,0:T(8,128)(2,1)}, u32[]{:S(2)}) copy-start(bf16[1024,1024]{1,0:T(8,128)(2,1)} %weight.1) | copy-start | bytes 6291460

commit v4 on v3

--- a/solution.py
+++ b/solution.py
@@ -170,14 +170,14 @@
     def near_mean(p):
         return pltpu.make_async_remote_copy(
             src_ref=near.at[p], dst_ref=near.at[p],
-            send_sem=m_send.at[n], recv_sem=m_recv.at[n + 1, p],
+            send_sem=m_send.at[n], recv_sem=m_recv.at[1, p],
             device_id={"kv": jnp.where(me == 1, first, last)}, device_id_type=MESH,
         )
 
     def near_level(g):
         return pltpu.make_async_remote_copy(
             src_ref=near_stat.at[g], dst_ref=near_stat.at[g],
-            send_sem=s_send.at[n], recv_sem=s_recv.at[n + 1, g],
+            send_sem=s_send.at[n], recv_sem=s_recv.at[1, g],
             device_id={"kv": jnp.where(me == 1, first, last)}, device_id_type=MESH,
         )
 
@@ -264,11 +264,6 @@
             else:
                 send_queries(chunk)
 
-    if reach:
-        @pl.when(jnp.logical_not(has_right))
-        def _():
-            send_queries(range(pairs))
-
     step_q = jnp.concatenate(step_q_parts, axis=1)
 
     c_gw.wait()
@@ -299,7 +294,8 @@
         if reach:
             for p in range(pairs):
                 q_to_far(p).start()
-        send_queries(range(pairs))
+        else:
+            send_queries(range(pairs))
 
     c_wk.wait()
     c_wv.wait()
@@ -437,12 +433,11 @@
             else:
                 q_to_left(me + k, p).wait_recv()
 
-    def relay(from_left, k, g):
+    def pass_on(from_left, k, g):
         for p in in_group(g):
-            if from_left:
-                q_to_right(me - k, p).start()
-            else:
-                q_to_left(me + k, p).start()
+            copy = q_to_right(me - k, p) if from_left else q_to_left(me + k, p)
+            copy.wait_recv()
+            copy.start()
 
     def attend_keep(from_left, k, g):
         source, used = (me - k, cache_len) if from_left else (me + k, keys)
@@ -532,6 +527,11 @@
 
     parts = len(groups)
 
+    if reach:
+        @pl.when(edge)
+        def _():
+            send_queries(range(pairs))
+
     def each_group(make):
         def body(g, carry):
             make(g)
@@ -562,18 +562,16 @@
                 fence()
                 decode()
 
-            @pl.when(i == max(1, n - 2))
-            def _():
-                @pl.when(has_left)
-                def _():
-                    pass_prefix()
-                    finish_bias()
-
-                attend_own()
-
             return carry
 
         lax.fori_loop(1, n, step, 0)
+
+        @pl.when(has_left)
+        def _():
+            pass_prefix()
+            finish_bias()
+
+        attend_own()
 
     if reach:
         @pl.when(me == n - 3)
@@ -581,18 +579,12 @@
             pass_prefix()
             finish_bias()
 
-            def turn_one(i, carry):
-                k = 2 - i
-
-                def body(g):
-                    arrived(False, k, g)
-                    relay(False, k, g)
+            def turn_one(g):
+                for k in (2, 1):
+                    pass_on(False, k, g)
                     attend_keep(False, k, g)
 
-                each_group(body)
-                return carry
-
-            lax.fori_loop(0, 2, turn_one, 0)
+            each_group(turn_one)
 
             def body(g):
                 arrived(True, 1, g)
@@ -602,22 +594,16 @@
 
         @pl.when(me == 2)
         def _():
-            def turn_two(i, carry):
-                k = 2 - i
-
-                def body(g):
-                    arrived(True, k, g)
-                    relay(True, k, g)
+            def turn_two(g):
+                for k in (2, 1):
+                    pass_on(True, k, g)
                     attend_keep(True, k, g)
 
-                    @pl.when(both(i == 0, g == 0))
-                    def _():
-                        pass_prefix()
-
-                each_group(body)
-                return carry
-
-            lax.fori_loop(0, 2, turn_two, 0)
+                @pl.when(g == 0)
+                def _():
+                    pass_prefix()
+
+            each_group(turn_two)
             finish_bias()
 
             def body(g):
@@ -636,8 +622,7 @@
                     @pl.when(there)
                     def _():
                         def body(g):
-                            arrived(from_left, k, g)
-                            relay(from_left, k, g)
+                            pass_on(from_left, k, g)
 
                         each_group(body)
 
@@ -883,7 +868,7 @@
             dma((17,)),
             dma((n,)), dma((n,)), dma(()), dma((n, pairs)),
             dma(()), dma(()), pltpu.SemaphoreType.REGULAR,
-            dma((n + 1,)), dma((n + 2, pairs)), dma((n + 1,)), dma((n + 2, groups)),
+            dma((n + 1,)), dma((n + 1, pairs)), dma((n + 1,)), dma((n + 1, groups)),
             dma(()), dma((pairs,)),
         ],
         compiler_params=pltpu.CompilerParams(

time: 28.4 us -> 28 us (0.986)
  Pallas kernels: 27 us -> 26.5 us
    pallas_call x1, Pallas kernels: 25.8 us -> 25.3 us  [per_device(): pl.pallas_call(functools.partial(kernel, n, heads, width), out_shape=pltp...]
where the time goes in v4:
time: 28 us; the launch traced here: 27.8 us
  Pallas kernels  26.5 us (95%)
  between operations  1.31 us (5%)
    pallas_call x1, Pallas kernels, per_device(): pl.pallas_call(functools.partial(kernel, n, heads, width), out_shape=pltp...  25.3 us
    pallas_call x1, Pallas kernels, per_device(): pl.pallas_call(functools.partial(project, rows), out_shape=(jax.ShapeDtyp...  1.19 us

profile of v4, /device:TPU:0, one launch (start us, length us, event | category | flops | bytes accessed | tf_op | source)
XLA Modules:
  0.0 27.8 jit_solution(14835733388615240119)
XLA Ops:
  1.3 0.0 copy-start
  1.3 25.3 %shard_map.176.att = bf16[144,1024]{1,0:T(8,128)(2,1)S(1)} custom-call(bf16[128,2048]{1,0:T(8,128)(2,1)} %tok_h.1, bf16[1,2048]{1,0:T(2,128)(2,1)} %stok_h.1, f32[1,2048]{1,0:T(1,128)} %bitcast.11, bf16[16,2048]{1,0:T(8,128)(2,1)} %bitcast.10, f32[1,16]{1,0:T(1,128)} %bitcast.12, f32[1,16]{1,0:T(1,128)} %bitcast.13, f32[8,512]{1,0:T(8,128)} %cache_decay_h.1, ...), custom_call_target="tpu_custom_call" | custom-call | tf_op jit(solution)/shard_map/pallas_call | solution.py:826
  26.6 0.0 copy-done
  26.7 1.2 %shard_map.177 = (bf16[128,1024]{1,0:T(8,128)(2,1)}, bf16[1,1024]{1,0:T(2,128)(2,1)}) custom-call(bf16[144,1024]{1,0:T(8,128)(2,1)S(1)} %shard_map.176.att, bf16[1024,1024]{1,0:T(8,128)(2,1)S(1)} %copy-done), custom_call_target="tpu_custom_call" | custom-call | tf_op jit(solution)/shard_map/pallas_call | solution.py:884
Async XLA Ops:
  1.3 25.4 %copy-start = (bf16[1024,1024]{1,0:T(8,128)(2,1)S(1)}, bf16[1024,1024]{1,0:T(8,128)(2,1)}, u32[]{:S(2)}) copy-start(bf16[1024,1024]{1,0:T(8,128)(2,1)} %weight.1) | copy-start | bytes 6291460

commit v5 on v4

--- a/solution.py
+++ b/solution.py
@@ -532,6 +532,10 @@
         def _():
             send_queries(range(pairs))
 
+    @pl.when(middle)
+    def _():
+        decode()
+
     def each_group(make):
         def body(g, carry):
             make(g)
@@ -638,8 +642,6 @@
     @pl.when(middle)
     def _():
         attend_own()
-        fence()
-        decode()
 
     def forward(side, owner):
         means, stats = (to_r, stat_r) if side == 0 else (to_l, stat_l)

time: 28 us -> 27.6 us (0.986)
  Pallas kernels: 26.5 us -> 26.2 us
    pallas_call x1, Pallas kernels: 25.3 us -> 25 us  [per_device(): pl.pallas_call(functools.partial(kernel, n, heads, width), out_shape=pltp...]
where the time goes in v5:
time: 27.6 us; the launch traced here: 27.5 us
  Pallas kernels  26.2 us (95%)
  between operations  1.31 us (5%)
    pallas_call x1, Pallas kernels, per_device(): pl.pallas_call(functools.partial(kernel, n, heads, width), out_shape=pltp...  25 us
    pallas_call x1, Pallas kernels, per_device(): pl.pallas_call(functools.partial(project, rows), out_shape=(jax.ShapeDtyp...  1.19 us

profile of v5, /device:TPU:0, one launch (start us, length us, event | category | flops | bytes accessed | tf_op | source)
XLA Modules:
  0.0 27.5 jit_solution(9366302039181355275)
XLA Ops:
  1.3 0.0 copy-start
  1.3 25.0 %shard_map.176.att = bf16[144,1024]{1,0:T(8,128)(2,1)S(1)} custom-call(bf16[128,2048]{1,0:T(8,128)(2,1)} %tok_h.1, bf16[1,2048]{1,0:T(2,128)(2,1)} %stok_h.1, f32[1,2048]{1,0:T(1,128)} %bitcast.11, bf16[16,2048]{1,0:T(8,128)(2,1)} %bitcast.10, f32[1,16]{1,0:T(1,128)} %bitcast.12, f32[1,16]{1,0:T(1,128)} %bitcast.13, f32[8,512]{1,0:T(8,128)} %cache_decay_h.1, ...), custom_call_target="tpu_custom_call" | custom-call | tf_op jit(solution)/shard_map/pallas_call | solution.py:828
  26.3 0.0 copy-done
  26.3 1.2 %shard_map.177 = (bf16[128,1024]{1,0:T(8,128)(2,1)}, bf16[1,1024]{1,0:T(2,128)(2,1)}) custom-call(bf16[144,1024]{1,0:T(8,128)(2,1)S(1)} %shard_map.176.att, bf16[1024,1024]{1,0:T(8,128)(2,1)S(1)} %copy-done), custom_call_target="tpu_custom_call" | custom-call | tf_op jit(solution)/shard_map/pallas_call | solution.py:886
Async XLA Ops:
  1.3 25.0 %copy-start = (bf16[1024,1024]{1,0:T(8,128)(2,1)S(1)}, bf16[1024,1024]{1,0:T(8,128)(2,1)}, u32[]{:S(2)}) copy-start(bf16[1024,1024]{1,0:T(8,128)(2,1)} %weight.1) | copy-start | bytes 6291460

commit v6 on v5

--- a/solution.py
+++ b/solution.py
@@ -234,6 +234,26 @@
             def _():
                 q_to_left(me, p).start()
 
+    def send_outward(which):
+        for p in which:
+            @pl.when(me == 1)
+            def _():
+                q_to_left(me, p).start()
+
+            @pl.when(me == n - 2)
+            def _():
+                q_to_right(me, p).start()
+
+    def send_inward(which):
+        for p in which:
+            @pl.when(me == 1)
+            def _():
+                q_to_right(me, p).start()
+
+            @pl.when(me == n - 2)
+            def _():
+                q_to_left(me, p).start()
+
     pairs_in_part = part // pair_lanes
     step_q_parts = []
     for c in range(halves):
@@ -255,7 +275,10 @@
             if reach:
                 @pl.when(has_right)
                 def _():
-                    send_queries(chunk)
+                    if c == 0 and halves > 1:
+                        send_queries(chunk)
+                    else:
+                        send_outward(chunk)
 
                 @pl.when(jnp.logical_not(has_right))
                 def _():
@@ -265,6 +288,13 @@
                 send_queries(chunk)
 
     step_q = jnp.concatenate(step_q_parts, axis=1)
+    if reach:
+        @pl.when(jnp.logical_not(has_left))
+        def _():
+            enter()
+            for p in range(pairs_in_part):
+                q_to_far(p).start()
+
 
     c_gw.wait()
     c_gb.wait()
@@ -285,14 +315,15 @@
         gate_in[...] = jnp.zeros(gate_in.shape, F32)
         gate_out[...] = own_sum
 
-        enter()
+        if not reach:
+            enter()
 
         @pl.when(has_right)
         def _():
             g_copy.start()
 
         if reach:
-            for p in range(pairs):
+            for p in range(pairs_in_part, pairs):
                 q_to_far(p).start()
         else:
             send_queries(range(pairs))
@@ -531,6 +562,10 @@
         @pl.when(edge)
         def _():
             send_queries(range(pairs))
+
+        @pl.when(middle)
+        def _():
+            send_inward(range(pairs_in_part if halves > 1 else 0, pairs))
 
     @pl.when(middle)
     def _():

time: 27.6 us -> 27.6 us (level)
  no operation moved by 1% of the time
where the time goes in v6:
time: 27.6 us; the launch traced here: 27.5 us
  Pallas kernels  26.2 us (95%)
  between operations  1.31 us (5%)
    pallas_call x1, Pallas kernels, per_device(): pl.pallas_call(functools.partial(kernel, n, heads, width), out_shape=pltp...  25 us
    pallas_call x1, Pallas kernels, per_device(): pl.pallas_call(functools.partial(project, rows), out_shape=(jax.ShapeDtyp...  1.19 us

profile of v6, /device:TPU:0, one launch (start us, length us, event | category | flops | bytes accessed | tf_op | source)
XLA Modules:
  0.0 27.5 jit_solution(2511929739220202953)
XLA Ops:
  1.3 0.0 copy-start
  1.3 25.0 %shard_map.176.att = bf16[144,1024]{1,0:T(8,128)(2,1)S(1)} custom-call(bf16[128,2048]{1,0:T(8,128)(2,1)} %tok_h.1, bf16[1,2048]{1,0:T(2,128)(2,1)} %stok_h.1, f32[1,2048]{1,0:T(1,128)} %bitcast.11, bf16[16,2048]{1,0:T(8,128)(2,1)} %bitcast.10, f32[1,16]{1,0:T(1,128)} %bitcast.12, f32[1,16]{1,0:T(1,128)} %bitcast.13, f32[8,512]{1,0:T(8,128)} %cache_decay_h.1, ...), custom_call_target="tpu_custom_call" | custom-call | tf_op jit(solution)/shard_map/pallas_call | solution.py:863
  26.3 0.0 copy-done
  26.3 1.2 %shard_map.177 = (bf16[128,1024]{1,0:T(8,128)(2,1)}, bf16[1,1024]{1,0:T(2,128)(2,1)}) custom-call(bf16[144,1024]{1,0:T(8,128)(2,1)S(1)} %shard_map.176.att, bf16[1024,1024]{1,0:T(8,128)(2,1)S(1)} %copy-done), custom_call_target="tpu_custom_call" | custom-call | tf_op jit(solution)/shard_map/pallas_call | solution.py:921
Async XLA Ops:
  1.3 25.0 %copy-start = (bf16[1024,1024]{1,0:T(8,128)(2,1)S(1)}, bf16[1024,1024]{1,0:T(8,128)(2,1)}, u32[]{:S(2)}) copy-start(bf16[1024,1024]{1,0:T(8,128)(2,1)} %weight.1) | copy-start | bytes 6291460
